TPU v7x, 256 devices: a whole 4x4x8 slice. The times are simulated.
256 devices in a mesh: fs: 32 (over z, x), rep: 4 (over y), tp: 2 (over core).
Axes of the slice: x: 4, y: 4, z: 8, core: 2. Of those that a mesh axis runs over, the one named last changes fastest.
Arguments:
- saved_input: bfloat16 [131072, 2048], P(('fs', 'rep')), may hold values from -24 to 24
- value_cotangent: bfloat16 [131072, 4096], P(('fs', 'rep'), 'tp'), may hold values from -0.0021972656 to 0.0021972656
- factor: bfloat16 [2048, 128], P('fs'), may hold values from -1.5 to 1.5
- weight: float32 [2048, 4096], P('fs', 'tp'), may hold values from -1.2 to 1.2
- first_moment: float32 [128, 4096], P('fs', 'tp'), may hold values from -1.8 to 1.8
- second_moment: float32 [128, 4096], P('fs', 'tp'), may hold values from 0.1 to 1
Outputs:
- low_grad: float32 [128, 4096], P('fs', 'tp')
- new_first: float32 [128, 4096], P('fs', 'tp')
- new_second: float32 [128, 4096], P('fs', 'tp')
- direction: float32 [2048, 4096], P('fs', 'tp')
- new_weight: float32 [2048, 4096], P('fs', 'tp')
- new_copy: bfloat16 [2048, 4096], P('fs', 'tp')
All inputs are finite; a program needn't handle non-finite values.
Results may differ from a plain program's by a relative error of at most 0.006.
Values may be sent and summed in bfloat16 or wider, within the bound.
A program may use at most 64 MiB of HBM per device.

v0:
```python
import jax
import jax.numpy as jnp
from jax import lax
from jax.sharding import PartitionSpec as P

D = 2048
E = 4096


first_decay = 0.9
second_decay = 0.9
learn_rate = 0.05
epsilon = 1e-08


def joined_along(blocks, dim):
    shape = list(blocks.shape[1:])
    shape[dim] *= blocks.shape[0]
    return jnp.moveaxis(blocks, 0, dim).reshape(shape)


def sent_to_all(shard, axis):
    size = lax.axis_size(axis)
    return lax.all_to_all(
        jnp.broadcast_to(shard[None], (size, *shard.shape)), axis, 0, 0, tiled=True
    )


def collect(shard, axis, dim):
    return joined_along(sent_to_all(shard, axis), dim)


def in_blocks(shard, dim, size):
    before, after = (shard.shape[:dim], shard.shape[dim + 1 :])
    return jnp.moveaxis(shard.reshape(*before, size, -1, *after), dim, 0)


def sum_at_owner(shard, axis, dim):
    blocks = in_blocks(shard, dim, lax.axis_size(axis))
    arrived = lax.all_to_all(blocks, axis, split_axis=0, concat_axis=0, tiled=True)
    return arrived.astype(jnp.float32).sum(axis=0)


def over_copies(shard, axis):
    everything = sent_to_all(shard, axis)
    return jnp.sum(everything, axis=0)


def on_device(saved_input, value_cotangent, factor, weight, first_moment, second_moment):
    factor_wide = factor.astype(jnp.float32)
    factor_whole = collect(factor, "fs", 0)
    projected = jnp.dot(saved_input, factor_whole, preferred_element_type=jnp.float32)
    upper = projected.astype(jnp.bfloat16)
    lower = (projected - upper.astype(jnp.float32)).astype(jnp.bfloat16)
    dims = (((0,), (0,)), ((), ()))
    high_part = lax.dot_general(upper, value_cotangent, dims, preferred_element_type=jnp.float32)
    low_part = lax.dot_general(lower, value_cotangent, dims, preferred_element_type=jnp.float32)
    low_grad = sum_at_owner((high_part + low_part).astype(jnp.bfloat16), "fs", 0)
    low_grad = over_copies(low_grad, "rep")
    new_first = first_decay * first_moment + (1.0 - first_decay) * low_grad
    new_second = second_decay * second_moment + (1.0 - second_decay) * low_grad * low_grad
    ratio = new_first / (jnp.sqrt(new_second) + epsilon)
    ratio_whole = collect(ratio, "fs", 0)
    raw = jnp.dot(factor_wide, ratio_whole, precision=lax.Precision.HIGHEST)
    total = over_copies(jnp.sum(raw * raw), ("fs", "tp"))
    spread = jnp.sqrt(total / (D * E))
    direction = raw / (spread + 1.0)
    new_weight = weight - learn_rate * direction
    return (low_grad, new_first, new_second, direction, new_weight, new_weight.astype(jnp.bfloat16))


def solution(mesh):
    placed = (
        P(("fs", "rep"), None),
        P(("fs", "rep"), "tp"),
        P("fs", None),
        P("fs", "tp"),
        P("fs", "tp"),
        P("fs", "tp"),
    )
    return jax.shard_map(
        on_device,
        mesh=mesh,
        in_specs=placed,
        out_specs=(
            P("fs", "tp"),
            P("fs", "tp"),
            P("fs", "tp"),
            P("fs", "tp"),
            P("fs", "tp"),
            P("fs", "tp"),
        ),
        check_vma=False,
    )
```

profile of v0, /device:TPU:1, one launch (start us, length us, event | category | flops | bytes accessed | tf_op | source)
XLA Modules:
  0.0 120.0 jit_solution(2271655297747339690)
XLA Ops:
  0.6 0.0 copy-start
  0.6 1.0 broadcast_in_dim.8
  1.6 28.1 %all_to_all.26 = bf16[32,64,128]{2,1,0:T(8,128)(2,1)S(1)} all-to-all(bf16[32,64,128]{2,1,0:T(8,128)(2,1)S(1)} %broadcast_in_dim.8), channel_id=1, replica_groups=mesh['fs'=32,'rep'=4,'tp'=2] {'fs'}, dimensions={0} | all-to-all | bytes 1048576 | tf_op jit(solution)/shard_map/all_to_all | solution.py:24
  29.7 3.4 %fusion.7 = f32[1024,128]{1,0:T(8,128)S(1)} fusion(bf16[1024,2048]{1,0:T(8,128)(2,1)} %param.6, bf16[2048,128]{1,0:T(8,128)(2,1)S(1)} %bitcast.10), kind=kOutput, calls=%fused_computation.15 | convolution fusion | flops 536870912 | bytes 5242880 | tf_op jit(solution)/shard_map/dot_general | solution.py:52
  33.1 0.7 fusion.2
  33.9 0.0 copy-start.4
  33.9 0.0 copy-start.5
  33.9 0.7 fusion
  34.7 0.0 copy-start.3
  34.7 0.2 reshape.28
  34.9 20.3 %all_to_all.27 = bf16[32,4,2048]{2,1,0:T(4,128)(2,1)S(1)} all-to-all(bf16[32,4,2048]{2,1,0:T(4,128)(2,1)S(1)} %reshape.28), channel_id=1, replica_groups=mesh['fs'=32,'rep'=4,'tp'=2] {'fs'}, dimensions={0} | all-to-all | bytes 1048576 | tf_op jit(solution)/shard_map/all_to_all | solution.py:40
  55.2 0.2 convert_reduce_fusion
  55.4 8.8 %all_to_all.28 = f32[4,4,2048]{2,1,0:T(4,128)S(1)} all-to-all(f32[4,4,2048]{2,1,0:T(4,128)S(1)} %broadcast_in_dim.9), channel_id=1, replica_groups=mesh['fs'=32,'rep'=4,'tp'=2] {'rep'}, dimensions={0} | all-to-all | bytes 262144 | tf_op jit(solution)/shard_map/all_to_all | solution.py:24
  64.3 0.0 copy-start.2
  64.3 0.7 add_divide_fusion
  65.0 0.2 broadcast_in_dim.10
  65.2 30.4 %all_to_all.29 = f32[32,4,2048]{2,1,0:T(4,128)S(1)} all-to-all(f32[32,4,2048]{2,1,0:T(4,128)S(1)} %broadcast_in_dim.10), channel_id=1, replica_groups=mesh['fs'=32,'rep'=4,'tp'=2] {'fs'}, dimensions={0} | all-to-all | bytes 2097152 | tf_op jit(solution)/shard_map/all_to_all | solution.py:24
  95.6 0.4 reshape.29
  96.0 0.0 copy-done.3
  96.0 1.2 multiply_reduce_fusion
  97.2 0.7 broadcast_in_dim.11
  97.9 19.6 %all_to_all.30 = f32[64,1,1]{2,1,0:T(1,128)S(1)} all-to-all(f32[64,1,1]{2,1,0:T(1,128)S(1)} %broadcast_in_dim.11), channel_id=1, replica_groups=mesh['fs'=32,'rep'=4,'tp'=2] {'fs','tp'}, dimensions={0} | all-to-all | bytes 512 | tf_op jit(solution)/shard_map/all_to_all | solution.py:24
  117.5 0.7 reduce_sum.39
  118.8 1.2 fusion.5
  (8 shorter events, 0.1 us)
Async XLA Ops:
  0.6 32.5 %copy-start = (bf16[1024,2048]{1,0:T(8,128)(2,1)S(1)}, bf16[1024,2048]{1,0:T(8,128)(2,1)}, u32[]{:S(2)}) copy-start(bf16[1024,2048]{1,0:T(8,128)(2,1)} %param.7) | copy-start | bytes 12582916
  33.9 30.4 %copy-start.4 = (f32[4,2048]{1,0:T(4,128)S(1)}, f32[4,2048]{1,0:T(4,128)}, u32[]{:S(2)}) copy-start(f32[4,2048]{1,0:T(4,128)} %param.11) | copy-start | bytes 98308
  33.9 30.4 %copy-start.5 = (f32[4,2048]{1,0:T(4,128)S(1)}, f32[4,2048]{1,0:T(4,128)}, u32[]{:S(2)}) copy-start(f32[4,2048]{1,0:T(4,128)} %param.10) | copy-start | bytes 98308
  34.7 61.3 %copy-start.3 = (bf16[64,128]{1,0:T(8,128)(2,1)S(1)}, bf16[64,128]{1,0:T(8,128)(2,1)}, u32[]{:S(2)}) copy-start(bf16[64,128]{1,0:T(8,128)(2,1)} %param.8) | copy-start | bytes 49156
  55.2 63.7 %copy-start.1 = (f32[64,2048]{1,0:T(8,128)S(1)}, f32[64,2048]{1,0:T(8,128)}, u32[]{:S(2)}) copy-start(f32[64,2048]{1,0:T(8,128)} %param.9) | copy-start | bytes 1572868
  64.3 55.7 %copy-start.2 = (f32[4,2048]{1,0:T(4,128)}, f32[4,2048]{1,0:T(4,128)S(1)}, u32[]{:S(2)}) copy-start(f32[4,2048]{1,0:T(4,128)S(1)} %reduce_sum.37) | copy-start | bytes 98308
where the time goes:
time: 120 us
  blocking collectives  107 us (89%)
  matrix products  6.11 us (5%)
  other arithmetic  2.74 us (2%)
  local copies, waits for them, and re-layouts  2.47 us (2%)
  between operations  1.46 us (1%)
    all_to_all x4, blocking collectives, sent_to_all(): lax.all_to_all(jnp.broadcast_to(shard[None], (size, *shard.shape)), axis,...  86.9 us
    all_to_all x1, blocking collectives, sum_at_owner(): lax.all_to_all(blocks, axis, split_axis=0, concat_axis=0, tiled=True)  20.3 us
    dot_general x1, matrix products, on_device(): jnp.dot(saved_input, factor_whole, preferred_element_type=jnp.float32)  3.43 us

commit v1 on v0

v1 whole, which is shorter than its diff:
```python
import functools

import jax
import jax.numpy as jnp
from jax import lax
from jax.experimental import pallas as pl
from jax.experimental.pallas import tpu as pltpu
from jax.sharding import PartitionSpec as P

MESH = pl.DeviceIdType.MESH
D = 2048
E = 4096
NX, NY, NZ = 4, 4, 8
PEERS = NX * NY
ROWS = 16
LANES = 128
OWNED = ROWS // NX
ZBLOCK = D // NZ
TOKENS = 1024
COLS = 2048
RANK = 128

first_decay = 0.9
second_decay = 0.9
learn_rate = 0.05
epsilon = 1e-08

PLANE = sorted(
    [(dx, dy) for dx in range(NX) for dy in range(NY) if (dx, dy) != (0, 0)],
    key=lambda d: -(min(d[0], NX - d[0]) + min(d[1], NY - d[1])),
)
Z_FAR = sorted(range(1, NZ), key=lambda d: -min(d, NZ - d))
Z_NEAR = [0] + Z_FAR[::-1]


def aligned(value, multiple):
    return pl.multiple_of(value * multiple, multiple)


def exchange_kernel(
    x_hbm, v_hbm, f_ref, fm_ref, sm_ref,
    rat_out, lg_out, tot_out,
    xv, vv, f_all, p_acc, pt, lsend, lrecv, zsend, zrecv, rat_all,
    mom_send, mom_recv, lg_send, lg_recv, tot_send, tot_recv,
    load_sem, out_sem, send_f, send_l, send_z, send_r, send_m, send_g, send_t,
    fz_sem, fxy_sem, lxy_sem, lz_sem, rz_sem, rxy_sem, m_sem, g_sem, t_sem,
):
    fs = lax.axis_index("fs")
    y = lax.axis_index("rep")
    tp = lax.axis_index("tp")
    x = lax.rem(fs, NX)
    z = lax.div(fs, NX)
    own = y * NX + x

    load_x = pltpu.make_async_copy(x_hbm, xv, load_sem.at[0])
    load_v = pltpu.make_async_copy(v_hbm, vv, load_sem.at[1])
    load_x.start()
    load_v.start()

    def plane_peer(dx, dy):
        px = lax.rem(x + dx, NX)
        py = lax.rem(y + dy, NY)
        return px, py, {"fs": z * NX + px, "rep": py}

    def z_peer(d):
        return {"fs": lax.rem(z + d, NZ) * NX + x}

    def send(src, dst, send_sem, recv_sem, device):
        pltpu.make_async_remote_copy(
            src_ref=src, dst_ref=dst, send_sem=send_sem, recv_sem=recv_sem,
            device_id=device, device_id_type=MESH,
        ).start()

    def drain(ref, sem):
        pltpu.make_async_copy(ref, ref, sem).wait()

    barrier = pltpu.get_barrier_semaphore()
    for d in Z_FAR:
        pl.semaphore_signal(barrier, inc=1, device_id=z_peer(d), device_id_type=MESH)
    for dx, dy in PLANE:
        pl.semaphore_signal(barrier, inc=1, device_id=plane_peer(dx, dy)[2], device_id_type=MESH)
    pl.semaphore_signal(barrier, inc=1, device_id={"tp": 1 - tp}, device_id_type=MESH)

    quarter = f_ref[pl.ds(aligned(y, ROWS), ROWS), :]
    f_own = pl.ds(aligned(z * PEERS + x * NY + y, ROWS), ROWS)
    f_all[f_own, :] = quarter
    for px in range(NX):
        cols = pl.ds(aligned(y * NX + px, LANES), LANES)
        mom_send[px, 0:OWNED, :] = fm_ref[:, cols]
        mom_send[px, OWNED:2 * OWNED, :] = sm_ref[:, cols]
    cols = pl.ds(aligned(own, LANES), LANES)
    mom_recv[x, 0:OWNED, :] = fm_ref[:, cols]
    mom_recv[x, OWNED:2 * OWNED, :] = sm_ref[:, cols]

    pl.semaphore_wait(barrier, NZ - 1 + PEERS - 1 + 1)

    for d in Z_FAR:
        send(f_all.at[f_own], f_all.at[f_own], send_f, fz_sem.at[NZ - d], z_peer(d))
    for d in Z_NEAR:
        zs = lax.rem(z + d, NZ)
        block = f_all.at[pl.ds(aligned(zs * PEERS + x * NY + y, ROWS), ROWS)]
        if d:
            drain(block, fz_sem.at[d])
        for dx, dy in PLANE:
            send(block, block, send_f, fxy_sem.at[d], plane_peer(dx, dy)[2])
    for dx in range(1, NX):
        px = lax.rem(x + dx, NX)
        send(mom_send.at[px], mom_recv.at[x], send_m, m_sem, {"fs": z * NX + px})

    load_x.wait()
    for step, d in enumerate(Z_NEAR):
        zs = lax.rem(z + d, NZ)
        rows = pl.ds(aligned(zs, ZBLOCK), ZBLOCK)
        drain(f_all.at[pl.ds(0, (PEERS - 1) * ROWS)], fxy_sem.at[d])
        term = jnp.dot(xv[:, rows], f_all[rows, :], preferred_element_type=jnp.float32)
        p_acc[...] = term if step == 0 else p_acc[...] + term
    projected = p_acc[...]
    upper = projected.astype(jnp.bfloat16)
    lower = (projected - upper.astype(jnp.float32)).astype(jnp.bfloat16)
    pt[0:RANK, :] = upper.T
    pt[RANK:, :] = lower.T

    load_v.wait()
    for dy in range(NY):
        py = lax.rem(y + NY - 1 - dy, NY)
        cols = pl.ds(aligned(py, NX * LANES), NX * LANES)
        both = jnp.dot(pt[...], vv[:, cols], preferred_element_type=jnp.float32)
        terms = (both[0:RANK] + both[RANK:]).astype(jnp.bfloat16)
        for zd in range(NZ):
            slot = lax.rem(zd - z + NZ, NZ)
            for px in range(NX):
                lsend[slot, py * NX + px] = terms[
                    zd * ROWS:(zd + 1) * ROWS, px * LANES:(px + 1) * LANES
                ]
    for d in Z_FAR + [0]:
        for dx, dy in PLANE:
            px, py, device = plane_peer(dx, dy)
            send(lsend.at[d, py * NX + px], lrecv.at[d, own], send_l, lxy_sem.at[d], device)

    whole = f_all[...]
    gram = lax.dot_general(whole, whole, (((0,), (0,)), ((), ())), preferred_element_type=jnp.float32)
    gram_1 = gram.astype(jnp.bfloat16)
    rest = gram - gram_1.astype(jnp.float32)
    gram_2 = rest.astype(jnp.bfloat16)
    gram_3 = (rest - gram_2.astype(jnp.float32)).astype(jnp.bfloat16)

    total = None
    for d in Z_FAR + [0]:
        drain(lrecv.at[d, pl.ds(0, PEERS - 1)], lxy_sem.at[d])
        lrecv[d, own] = lsend[d, own]
        summed = jnp.sum(lrecv[d].astype(jnp.float32), axis=0)
        if d:
            zsend[d] = summed.astype(jnp.bfloat16)
            send(zsend.at[d], zrecv.at[NZ - d], send_z, lz_sem.at[NZ - d], z_peer(d))
        else:
            total = summed
    for d in Z_NEAR[1:]:
        drain(zrecv.at[d], lz_sem.at[d])
        total = total + zrecv[d].astype(jnp.float32)

    drain(mom_recv.at[pl.ds(0, NX - 1)], m_sem)
    first = jnp.concatenate([mom_recv[i, 0:OWNED, :] for i in range(NX)], axis=0)
    second = jnp.concatenate([mom_recv[i, OWNED:2 * OWNED, :] for i in range(NX)], axis=0)
    new_first = first_decay * first + (1.0 - first_decay) * total
    new_second = second_decay * second + (1.0 - second_decay) * total * total
    ratio = new_first / (jnp.sqrt(new_second) + epsilon)
    tile_cols = pl.ds(aligned(own, LANES), LANES)
    rat_all[pl.ds(aligned(z, ROWS), ROWS), tile_cols] = ratio.astype(jnp.bfloat16)
    for i in range(NX):
        lg_send[i, 0:OWNED, :] = total[i * OWNED:(i + 1) * OWNED, :]
    lg_recv[own, 0:OWNED, :] = lg_send[x, 0:OWNED, :]

    tile = rat_all.at[pl.ds(aligned(z, ROWS), ROWS), tile_cols]
    for d in Z_FAR:
        send(tile, tile, send_r, rz_sem.at[NZ - d], z_peer(d))
    for d in Z_NEAR:
        zs = lax.rem(z + d, NZ)
        block = rat_all.at[pl.ds(aligned(zs, ROWS), ROWS), tile_cols]
        if d:
            drain(block, rz_sem.at[d])
        for dx, dy in PLANE:
            send(block, block, send_r, rxy_sem.at[d], plane_peer(dx, dy)[2])
    for dx, dy in PLANE:
        px, py, device = plane_peer(dx, dy)
        send(lg_send.at[px], lg_recv.at[own], send_g, g_sem, device)
    for d in Z_NEAR:
        drain(lrecv.at[d, pl.ds(0, PEERS - 1)], rxy_sem.at[d])

    ratio_whole = rat_all[...]
    squares = jnp.zeros((8, LANES), jnp.float32)
    for c in range(COLS // 512):
        part = ratio_whole[:, c * 512:(c + 1) * 512]
        mixed = (
            jnp.dot(gram_1, part, preferred_element_type=jnp.float32)
            + jnp.dot(gram_2, part, preferred_element_type=jnp.float32)
            + jnp.dot(gram_3, part, preferred_element_type=jnp.float32)
        ) * part.astype(jnp.float32)
        for k in range(4):
            squares = squares + jnp.sum(
                mixed[:, k * LANES:(k + 1) * LANES].reshape(RANK // 8, 8, LANES), axis=0
            )
    tot_send[...] = squares
    send(tot_send, tot_recv, send_t, t_sem, {"tp": 1 - tp})
    save = pltpu.make_async_copy(rat_all, rat_out, out_sem)
    save.start()
    drain(lg_recv.at[pl.ds(0, PEERS - 1)], g_sem)
    lg_out[...] = lg_recv[...]
    drain(tot_recv, t_sem)
    tot_out[...] = squares + tot_recv[...]

    save.wait()
    drain(f_all.at[pl.ds(0, (NZ - 1) * ROWS)], send_f)
    for d in range(NZ):
        drain(f_all.at[pl.ds(0, (PEERS - 1) * ROWS)], send_f)
    drain(lsend.at[:, pl.ds(0, PEERS - 1)], send_l)
    drain(zsend.at[pl.ds(0, NZ - 1)], send_z)
    drain(zsend.at[pl.ds(0, NZ - 1)], send_r)
    drain(lsend.at[:, pl.ds(0, PEERS - 1)], send_r)
    drain(mom_send.at[pl.ds(0, NX - 1)], send_m)
    drain(lg_recv.at[pl.ds(0, PEERS - 1)], send_g)
    drain(tot_send, send_t)


def exchange(saved_input, value_cotangent, factor, first_moment, second_moment):
    bf16, f32 = jnp.bfloat16, jnp.float32
    dma = pltpu.SemaphoreType.DMA
    vmem = pl.BlockSpec(memory_space=pltpu.VMEM)
    hbm = pl.BlockSpec(memory_space=pl.ANY)
    return pl.pallas_call(
        exchange_kernel,
        out_shape=(
            jax.ShapeDtypeStruct((RANK, COLS), bf16),
            jax.ShapeDtypeStruct((PEERS, 8, LANES), f32),
            jax.ShapeDtypeStruct((8, LANES), f32),
        ),
        in_specs=[hbm, hbm, vmem, vmem, vmem],
        out_specs=(hbm, vmem, vmem),
        scratch_shapes=[
            pltpu.VMEM((TOKENS, D), bf16),
            pltpu.VMEM((TOKENS, COLS), bf16),
            pltpu.VMEM((D, RANK), bf16),
            pltpu.VMEM((TOKENS, RANK), f32),
            pltpu.VMEM((2 * RANK, TOKENS), bf16),
            pltpu.VMEM((NZ, PEERS, ROWS, LANES), bf16),
            pltpu.VMEM((NZ, PEERS, ROWS, LANES), bf16),
            pltpu.VMEM((NZ, ROWS, LANES), bf16),
            pltpu.VMEM((NZ, ROWS, LANES), bf16),
            pltpu.VMEM((RANK, COLS), bf16),
            pltpu.VMEM((NX, 8, LANES), f32),
            pltpu.VMEM((NX, 8, LANES), f32),
            pltpu.VMEM((NX, 8, LANES), f32),
            pltpu.VMEM((PEERS, 8, LANES), f32),
            pltpu.VMEM((8, LANES), f32),
            pltpu.VMEM((8, LANES), f32),
            dma((2,)),
        ] + [dma] * 8 + [dma((NZ,))] * 6 + [dma] * 3,
        compiler_params=pltpu.CompilerParams(
            collective_id=0, has_side_effects=True, vmem_limit_bytes=40 * 2**20
        ),
    )(saved_input, value_cotangent, factor, first_moment, second_moment)


def update_kernel(
    f_ref, rat_ref, lg_ref, tot_ref, w_ref, fm_ref, sm_ref,
    low_ref, first_ref, second_ref, dir_ref, weight_ref, copy_ref,
):
    total = jnp.sum(tot_ref[...], axis=(0, 1), keepdims=True)
    spread = jnp.sqrt(total / (D * E))
    raw = jnp.dot(f_ref[...], rat_ref[...], preferred_element_type=jnp.float32)
    direction = raw / (spread + 1.0)
    new_weight = w_ref[...] - learn_rate * direction
    dir_ref[...] = direction
    weight_ref[...] = new_weight
    copy_ref[...] = new_weight.astype(jnp.bfloat16)
    for j in range(PEERS):
        cols = slice(j * LANES, (j + 1) * LANES)
        low = lg_ref[j, 0:OWNED, :]
        low_ref[:, cols] = low
        first_ref[:, cols] = first_decay * fm_ref[:, cols] + (1.0 - first_decay) * low
        second_ref[:, cols] = second_decay * sm_ref[:, cols] + (1.0 - second_decay) * low * low


def update(factor, ratio, low, total, weight, first_moment, second_moment):
    f32 = jnp.float32
    rows = factor.shape[0]
    vmem = pl.BlockSpec(memory_space=pltpu.VMEM)
    small = jax.ShapeDtypeStruct((OWNED, COLS), f32)
    large = jax.ShapeDtypeStruct((rows, COLS), f32)
    return pl.pallas_call(
        update_kernel,
        out_shape=(small, small, small, large, large, jax.ShapeDtypeStruct((rows, COLS), jnp.bfloat16)),
        in_specs=[vmem] * 7,
        out_specs=(vmem,) * 6,
    )(factor, ratio, low, total, weight, first_moment, second_moment)


def on_device(saved_input, value_cotangent, factor, weight, first_moment, second_moment):
    ratio, low, total = exchange(saved_input, value_cotangent, factor, first_moment, second_moment)
    return update(factor, ratio, low, total, weight, first_moment, second_moment)


def solution(mesh):
    placed = (
        P(("fs", "rep"), None),
        P(("fs", "rep"), "tp"),
        P("fs", None),
        P("fs", "tp"),
        P("fs", "tp"),
        P("fs", "tp"),
    )
    return jax.shard_map(
        on_device,
        mesh=mesh,
        in_specs=placed,
        out_specs=(P("fs", "tp"),) * 6,
        check_vma=False,
    )
```

time: 120 us -> 59.2 us (0.49)
  blocking collectives: 107 us -> 0 us
  Pallas kernels: 0 us -> 49.6 us
  local copies, waits for them, and re-layouts: 2.47 us -> 8.61 us
  matrix products: 6.11 us -> 0 us
  other arithmetic: 2.74 us -> 0 us
    all_to_all x5 -> x0, blocking collectives: 107 us -> none  [the longest x4 86.9 us: sent_to_all(): lax.all_to_all(jnp.broadcast_to(shard[None], (size, *shard.shape)), axis,...]
    pallas_call x0 -> x2, Pallas kernels: none -> 49.6 us  [the longest x1 47 us: exchange(): pl.pallas_call(exchange_kernel, out_shape=(jax.ShapeDtypeStruct((RANK, CO...]
    unnamed x12 -> x16, local copies, waits for them, and re-layouts: 0.03 us -> 8.61 us
    dot_general x4 -> x0, matrix products: 6.11 us -> none  [the longest x1 3.43 us: on_device(): jnp.dot(saved_input, factor_whole, preferred_element_type=jnp.float32)]
    broadcast_in_dim x4 -> x0, local copies, waits for them, and re-layouts: 1.88 us -> none  [sent_to_all(): jnp.broadcast_to(shard[None], (size, *shard.shape))]
where the time goes in v1:
time: 59.2 us; the launch traced here: 58.8 us
  Pallas kernels  49.6 us (84%)
  local copies, waits for them, and re-layouts  8.61 us (15%)
  between operations  0.66 us (1%)
    pallas_call x1, Pallas kernels, exchange(): pl.pallas_call(exchange_kernel, out_shape=(jax.ShapeDtypeStruct((RANK, CO...  47 us
    unnamed x16, local copies, waits for them, and re-layouts  8.61 us
    pallas_call x1, Pallas kernels, update(): pl.pallas_call(update_kernel, out_shape=(small, small, small, large, larg...  2.57 us

profile of v1, /device:TPU:1, one launch (start us, length us, event | category | flops | bytes accessed | tf_op | source)
XLA Modules:
  0.0 58.8 jit_solution(12679261656077523273)
XLA Ops:
  0.6 0.0 copy-start
  0.6 2.2 %copy-done = bf16[1024,2048]{1,0:T(8,128)(2,1)S(1)} copy-done((bf16[1024,2048]{1,0:T(8,128)(2,1)S(1)}, bf16[1024,2048]{1,0:T(8,128)(2,1)}, u32[]{:S(2)}) %copy-start) | copy-done | bytes 4194328
  2.8 0.0 copy-start.1
  2.8 2.2 %copy-done.1 = bf16[1024,2048]{1,0:T(8,128)(2,1)S(1)} copy-done((bf16[1024,2048]{1,0:T(8,128)(2,1)S(1)}, bf16[1024,2048]{1,0:T(8,128)(2,1)}, u32[]{:S(2)}) %copy-start.1) | copy-done | bytes 4194328
  5.0 0.0 copy-start.3
  5.0 0.8 %copy-done.3 = f32[4,2048]{1,0:T(4,128)S(1)} copy-done((f32[4,2048]{1,0:T(4,128)S(1)}, f32[4,2048]{1,0:T(4,128)}, u32[]{:S(2)}) %copy-start.3) | copy-done | bytes 32792
  5.8 0.0 copy-start.4
  5.8 0.8 %copy-done.4 = f32[4,2048]{1,0:T(4,128)S(1)} copy-done((f32[4,2048]{1,0:T(4,128)S(1)}, f32[4,2048]{1,0:T(4,128)}, u32[]{:S(2)}) %copy-start.4) | copy-done | bytes 32792
  6.5 0.0 copy-start.5
  6.5 0.7 %copy-done.5 = bf16[64,128]{1,0:T(8,128)(2,1)S(1)} copy-done((bf16[64,128]{1,0:T(8,128)(2,1)S(1)}, bf16[64,128]{1,0:T(8,128)(2,1)}, u32[]{:S(2)}) %copy-start.5) | copy-done | bytes 16408
  7.2 47.0 %shard_map.109 = (bf16[128,2048]{1,0:T(8,128)(2,1)S(1)}, f32[16,8,128]{2,1,0:T(8,128)S(1)}, f32[8,128]{1,0:T(8,128)S(1)}) custom-call(bf16[1024,2048]{1,0:T(8,128)(2,1)S(1)} %copy-done, bf16[1024,2048]{1,0:T(8,128)(2,1)S(1)} %copy-done.1, bf16[64,128]{1,0:T(8,128)(2,1)S(1)} %copy-done.5, f32[4,2048]{1,0:T(4,128)S(1)} %copy-done.3, f32[4,2048]{1,0:T(4,128)S(1)} %copy-done.4), custom_call_target="tpu_custom_call" | custom-call | tf_op jit(solution)/shard_map/pallas_call | solution.py:229
  54.2 0.0 copy-start.2
  54.3 0.8 %copy-done.2 = bf16[128,2048]{1,0:T(8,128)(2,1)} copy-done((bf16[128,2048]{1,0:T(8,128)(2,1)}, bf16[128,2048]{1,0:T(8,128)(2,1)S(1)}, u32[]{:S(2)}) %copy-start.2) | copy-done | bytes 524312
  55.1 0.0 copy-start.6
  55.1 0.6 %copy-done.6 = f32[16,8,128]{2,1,0:T(8,128)} copy-done((f32[16,8,128]{2,1,0:T(8,128)}, f32[16,8,128]{2,1,0:T(8,128)S(1)}, u32[]{:S(2)}) %copy-start.6) | copy-done | bytes 65560
  55.7 0.0 copy-start.7
  55.7 0.6 %copy-done.7 = f32[8,128]{1,0:T(8,128)} copy-done((f32[8,128]{1,0:T(8,128)}, f32[8,128]{1,0:T(8,128)S(1)}, u32[]{:S(2)}) %copy-start.7) | copy-done | bytes 4120
  56.3 2.6 %shard_map.110 = (f32[4,2048]{1,0:T(4,128)}, f32[4,2048]{1,0:T(4,128)}, f32[4,2048]{1,0:T(4,128)}, f32[64,2048]{1,0:T(8,128)}, f32[64,2048]{1,0:T(8,128)}, /*index=5*/bf16[64,2048]{1,0:T(8,128)(2,1)}) custom-call(bf16[64,128]{1,0:T(8,128)(2,1)} %f_ref.3, bf16[128,2048]{1,0:T(8,128)(2,1)} %copy-done.2, f32[16,8,128]{2,1,0:T(8,128)} %copy-done.6, ...), custom_call_target="tpu_custom_call" | custom-call | tf_op jit(solution)/shard_map/pallas_call | solution.py:289
Async XLA Ops:
  0.6 2.2 %copy-start = (bf16[1024,2048]{1,0:T(8,128)(2,1)S(1)}, bf16[1024,2048]{1,0:T(8,128)(2,1)}, u32[]{:S(2)}) copy-start(bf16[1024,2048]{1,0:T(8,128)(2,1)} %x_hbm.1) | copy-start | bytes 12582916
  2.8 2.2 %copy-start.1 = (bf16[1024,2048]{1,0:T(8,128)(2,1)S(1)}, bf16[1024,2048]{1,0:T(8,128)(2,1)}, u32[]{:S(2)}) copy-start(bf16[1024,2048]{1,0:T(8,128)(2,1)} %v_hbm.1) | copy-start | bytes 12582916
  5.0 0.8 %copy-start.3 = (f32[4,2048]{1,0:T(4,128)S(1)}, f32[4,2048]{1,0:T(4,128)}, u32[]{:S(2)}) copy-start(f32[4,2048]{1,0:T(4,128)} %fm_ref.3) | copy-start | bytes 98308
  5.8 0.8 %copy-start.4 = (f32[4,2048]{1,0:T(4,128)S(1)}, f32[4,2048]{1,0:T(4,128)}, u32[]{:S(2)}) copy-start(f32[4,2048]{1,0:T(4,128)} %sm_ref.3) | copy-start | bytes 98308
  6.5 0.7 %copy-start.5 = (bf16[64,128]{1,0:T(8,128)(2,1)S(1)}, bf16[64,128]{1,0:T(8,128)(2,1)}, u32[]{:S(2)}) copy-start(bf16[64,128]{1,0:T(8,128)(2,1)} %f_ref.3) | copy-start | bytes 49156
  54.2 0.8 %copy-start.2 = (bf16[128,2048]{1,0:T(8,128)(2,1)}, bf16[128,2048]{1,0:T(8,128)(2,1)S(1)}, u32[]{:S(2)}) copy-start(bf16[128,2048]{1,0:T(8,128)(2,1)S(1)} %get-tuple-element.9.rat_ref) | copy-start | bytes 1572868
  55.1 0.6 %copy-start.6 = (f32[16,8,128]{2,1,0:T(8,128)}, f32[16,8,128]{2,1,0:T(8,128)S(1)}, u32[]{:S(2)}) copy-start(f32[16,8,128]{2,1,0:T(8,128)S(1)} %get-tuple-element.10.lg_ref) | copy-start | bytes 196612
  55.7 0.6 %copy-start.7 = (f32[8,128]{1,0:T(8,128)}, f32[8,128]{1,0:T(8,128)S(1)}, u32[]{:S(2)}) copy-start(f32[8,128]{1,0:T(8,128)S(1)} %get-tuple-element.11.tot_ref) | copy-start | bytes 12292

commit v2 on v1

--- a/solution.py
+++ b/solution.py
@@ -38,11 +38,11 @@
 
 
 def exchange_kernel(
-    x_hbm, v_hbm, f_ref, fm_ref, sm_ref,
+    x_hbm, v_hbm, f_hbm, fm_hbm, sm_hbm,
     rat_out, lg_out, tot_out,
-    xv, vv, f_all, p_acc, pt, lsend, lrecv, zsend, zrecv, rat_all,
+    f_ref, fm_ref, sm_ref, xv, vv, f_all, p_acc, pt, lsend, lrecv, zsend, zrecv, rat_all,
     mom_send, mom_recv, lg_send, lg_recv, tot_send, tot_recv,
-    load_sem, out_sem, send_f, send_l, send_z, send_r, send_m, send_g, send_t,
+    load_sem, send_f, send_l, send_z, send_r, send_m, send_g, send_t,
     fz_sem, fxy_sem, lxy_sem, lz_sem, rz_sem, rxy_sem, m_sem, g_sem, t_sem,
 ):
     fs = lax.axis_index("fs")
@@ -52,10 +52,13 @@
     z = lax.div(fs, NX)
     own = y * NX + x
 
+    load_f = pltpu.make_async_copy(f_hbm, f_ref, load_sem.at[2])
+    load_fm = pltpu.make_async_copy(fm_hbm, fm_ref, load_sem.at[3])
+    load_sm = pltpu.make_async_copy(sm_hbm, sm_ref, load_sem.at[4])
     load_x = pltpu.make_async_copy(x_hbm, xv, load_sem.at[0])
     load_v = pltpu.make_async_copy(v_hbm, vv, load_sem.at[1])
-    load_x.start()
-    load_v.start()
+    for load in (load_f, load_fm, load_sm, load_x, load_v):
+        load.start()
 
     def plane_peer(dx, dy):
         px = lax.rem(x + dx, NX)
@@ -81,6 +84,9 @@
         pl.semaphore_signal(barrier, inc=1, device_id=plane_peer(dx, dy)[2], device_id_type=MESH)
     pl.semaphore_signal(barrier, inc=1, device_id={"tp": 1 - tp}, device_id_type=MESH)
 
+    load_f.wait()
+    load_fm.wait()
+    load_sm.wait()
     quarter = f_ref[pl.ds(aligned(y, ROWS), ROWS), :]
     f_own = pl.ds(aligned(z * PEERS + x * NY + y, ROWS), ROWS)
     f_all[f_own, :] = quarter
@@ -201,14 +207,12 @@
             )
     tot_send[...] = squares
     send(tot_send, tot_recv, send_t, t_sem, {"tp": 1 - tp})
-    save = pltpu.make_async_copy(rat_all, rat_out, out_sem)
-    save.start()
+    rat_out[...] = ratio_whole
     drain(lg_recv.at[pl.ds(0, PEERS - 1)], g_sem)
     lg_out[...] = lg_recv[...]
     drain(tot_recv, t_sem)
     tot_out[...] = squares + tot_recv[...]
 
-    save.wait()
     drain(f_all.at[pl.ds(0, (NZ - 1) * ROWS)], send_f)
     for d in range(NZ):
         drain(f_all.at[pl.ds(0, (PEERS - 1) * ROWS)], send_f)
@@ -225,7 +229,7 @@
     bf16, f32 = jnp.bfloat16, jnp.float32
     dma = pltpu.SemaphoreType.DMA
     vmem = pl.BlockSpec(memory_space=pltpu.VMEM)
-    hbm = pl.BlockSpec(memory_space=pl.ANY)
+    hbm = pl.BlockSpec(memory_space=pltpu.HBM)
     return pl.pallas_call(
         exchange_kernel,
         out_shape=(
@@ -233,9 +237,12 @@
             jax.ShapeDtypeStruct((PEERS, 8, LANES), f32),
             jax.ShapeDtypeStruct((8, LANES), f32),
         ),
-        in_specs=[hbm, hbm, vmem, vmem, vmem],
-        out_specs=(hbm, vmem, vmem),
+        in_specs=[hbm] * 5,
+        out_specs=(vmem,) * 3,
         scratch_shapes=[
+            pltpu.VMEM((D // (NX * NZ), RANK), bf16),
+            pltpu.VMEM((OWNED, COLS), f32),
+            pltpu.VMEM((OWNED, COLS), f32),
             pltpu.VMEM((TOKENS, D), bf16),
             pltpu.VMEM((TOKENS, COLS), bf16),
             pltpu.VMEM((D, RANK), bf16),
@@ -252,12 +259,15 @@
             pltpu.VMEM((PEERS, 8, LANES), f32),
             pltpu.VMEM((8, LANES), f32),
             pltpu.VMEM((8, LANES), f32),
-            dma((2,)),
-        ] + [dma] * 8 + [dma((NZ,))] * 6 + [dma] * 3,
+            dma((5,)),
+        ] + [dma] * 7 + [dma((NZ,))] * 6 + [dma] * 3,
         compiler_params=pltpu.CompilerParams(
-            collective_id=0, has_side_effects=True, vmem_limit_bytes=40 * 2**20
+            collective_id=0, has_side_effects=True, vmem_limit_bytes=32 * 2**20
         ),
-    )(saved_input, value_cotangent, factor, first_moment, second_moment)
+    )(*(
+        pltpu.with_memory_space_constraint(a, pltpu.HBM)
+        for a in (saved_input, value_cotangent, factor, first_moment, second_moment)
+    ))
 
 
 def update_kernel(
@@ -291,6 +301,7 @@
         out_shape=(small, small, small, large, large, jax.ShapeDtypeStruct((rows, COLS), jnp.bfloat16)),
         in_specs=[vmem] * 7,
         out_specs=(vmem,) * 6,
+        compiler_params=pltpu.CompilerParams(vmem_limit_bytes=8 * 2**20),
     )(factor, ratio, low, total, weight, first_moment, second_moment)
 
 

time: 59.2 us -> 48.7 us (0.82)
  local copies, waits for them, and re-layouts: 8.61 us -> 0.02 us
  Pallas kernels: 49.6 us -> 47.9 us
    unnamed x16 -> x8, local copies, waits for them, and re-layouts: 8.61 us -> 0.02 us
    pallas_call x1, Pallas kernels: 2.57 us -> 1.31 us  [update(): pl.pallas_call(update_kernel, out_shape=(small, small, small, large, larg...]
where the time goes in v2:
time: 48.7 us; the launch traced here: 48.6 us
  Pallas kernels  47.9 us (98%)
  between operations  0.7 us (1%)
    pallas_call x1, Pallas kernels, exchange(): pl.pallas_call(exchange_kernel, out_shape=(jax.ShapeDtypeStruct((RANK, CO...  46.6 us
    pallas_call x1, Pallas kernels, update(): pl.pallas_call(update_kernel, out_shape=(small, small, small, large, larg...  1.31 us

profile of v2, /device:TPU:1, one launch (start us, length us, event | category | flops | bytes accessed | tf_op | source)
XLA Modules:
  0.0 48.6 jit_solution(5578171237300622040)
XLA Ops:
  0.6 0.0 copy-start.2
  0.6 0.0 copy-start.1
  0.7 0.0 copy-start.3
  0.7 0.0 copy-start
  0.7 46.6 %shard_map.109 = (bf16[128,2048]{1,0:T(8,128)(2,1)S(1)}, f32[16,8,128]{2,1,0:T(8,128)S(1)}, f32[8,128]{1,0:T(8,128)S(1)}) custom-call(bf16[1024,2048]{1,0:T(8,128)(2,1)} %x_hbm.1, bf16[1024,2048]{1,0:T(8,128)(2,1)} %v_hbm.1, bf16[64,128]{1,0:T(8,128)(2,1)} %f_ref.1, f32[4,2048]{1,0:T(4,128)} %fm_ref.1, f32[4,2048]{1,0:T(4,128)} %sm_ref.1), custom_call_target="tpu_custom_call" | custom-call | tf_op jit(solution)/shard_map/pallas_call | solution.py:233
  47.3 0.0 copy-done.2
  47.3 0.0 copy-done.1
  47.3 0.0 copy-done.3
  47.3 0.0 copy-done
  47.3 1.3 %shard_map.110 = (f32[4,2048]{1,0:T(4,128)}, f32[4,2048]{1,0:T(4,128)}, f32[4,2048]{1,0:T(4,128)}, f32[64,2048]{1,0:T(8,128)}, f32[64,2048]{1,0:T(8,128)}, /*index=5*/bf16[64,2048]{1,0:T(8,128)(2,1)}) custom-call(bf16[64,128]{1,0:T(8,128)(2,1)S(1)} %copy-done.3, bf16[128,2048]{1,0:T(8,128)(2,1)S(1)} %get-tuple-element.9.rat_ref, ...), custom_call_target="tpu_custom_call" | custom-call | tf_op jit(solution)/shard_map/pallas_call | solution.py:299
Async XLA Ops:
  0.6 46.7 %copy-start.2 = (f32[4,2048]{1,0:T(4,128)S(1)}, f32[4,2048]{1,0:T(4,128)}, u32[]{:S(2)}) copy-start(f32[4,2048]{1,0:T(4,128)} %sm_ref.1) | copy-start | bytes 98308
  0.6 46.7 %copy-start.1 = (f32[4,2048]{1,0:T(4,128)S(1)}, f32[4,2048]{1,0:T(4,128)}, u32[]{:S(2)}) copy-start(f32[4,2048]{1,0:T(4,128)} %fm_ref.1) | copy-start | bytes 98308
  0.7 46.7 %copy-start.3 = (bf16[64,128]{1,0:T(8,128)(2,1)S(1)}, bf16[64,128]{1,0:T(8,128)(2,1)}, u32[]{:S(2)}) copy-start(bf16[64,128]{1,0:T(8,128)(2,1)} %f_ref.1) | copy-start | bytes 49156
  0.7 46.7 %copy-start = (f32[64,2048]{1,0:T(8,128)S(1)}, f32[64,2048]{1,0:T(8,128)}, u32[]{:S(2)}) copy-start(f32[64,2048]{1,0:T(8,128)} %w_ref.1) | copy-start | bytes 1572868

commit v3 on v2

v3 whole, which is shorter than its diff:
```python
import functools

import jax
import jax.numpy as jnp
from jax import lax
from jax.experimental import pallas as pl
from jax.experimental.pallas import tpu as pltpu
from jax.sharding import PartitionSpec as P

MESH = pl.DeviceIdType.MESH
D = 2048
E = 4096
NX, NY, NZ = 4, 4, 8
PEERS = NX * NY
ROWS = 16
LANES = 128
OWNED = ROWS // NX
ZBLOCK = D // NZ
TOKENS = 1024
COLS = 2048
RANK = 128

first_decay = 0.9
second_decay = 0.9
learn_rate = 0.05
epsilon = 1e-08

PLANE = sorted(
    [(dx, dy) for dx in range(NX) for dy in range(NY) if (dx, dy) != (0, 0)],
    key=lambda d: -(min(d[0], NX - d[0]) + min(d[1], NY - d[1])),
)
Z_FAR = [4, 3, 5, 2, 6, 1, 7]
GROUPS = [(0,), (1, 7), (2, 6), (3, 5), (4,)]
BASE = [PEERS * sum(len(g) for g in GROUPS[:i]) for i in range(len(GROUPS))]
GROUP_OF = {d: (i, k) for i, g in enumerate(GROUPS) for k, d in enumerate(g)}
PARTS = [(4, 3, 5), (2, 6, 1, 7, 0)]
ORDER = [d for part in PARTS for d in part]
NEAR = [0, 3, 1, 2]


def aligned(value, multiple):
    return pl.multiple_of(value * multiple, multiple)


def exchange_kernel(
    x_hbm, v_hbm, f_hbm, fm_hbm, sm_hbm,
    rat_out, lg_out, tot_out,
    f_ref, fm_ref, sm_ref, xv, vv, fbuf, p_acc, pt, lsend, lrecv, zsend, zrecv, rbuf, column,
    mom_send, mom_recv, lg_send, lg_recv, square, squares,
    load_sem, send_f, send_l, send_z, send_r, send_m, send_g, send_q,
    fz_sem, fxy_sem, lxy_sem, lz_sem, rz_sem, rxy_sem, m_sem, g_sem, q_sem,
):
    fs = lax.axis_index("fs")
    y = lax.axis_index("rep")
    tp = lax.axis_index("tp")
    x = lax.rem(fs, NX)
    z = lax.div(fs, NX)
    own = y * NX + x
    own_f = x * NY + y

    def plane_peer(dx, dy):
        px = lax.rem(x + dx, NX)
        py = lax.rem(y + dy, NY)
        return px, py, {"fs": z * NX + px, "rep": py}

    def z_peer(d):
        return {"fs": lax.rem(z + d, NZ) * NX + x}

    def send(src, dst, send_sem, recv_sem, device):
        pltpu.make_async_remote_copy(
            src_ref=src, dst_ref=dst, send_sem=send_sem, recv_sem=recv_sem,
            device_id=device, device_id_type=MESH,
        ).start()

    def drain(ref, sem):
        pltpu.make_async_copy(ref, ref, sem).wait()

    barrier = pltpu.get_barrier_semaphore()
    for d in Z_FAR:
        pl.semaphore_signal(barrier, inc=1, device_id=z_peer(d), device_id_type=MESH)
    for dx, dy in PLANE:
        device = plane_peer(dx, dy)[2]
        pl.semaphore_signal(barrier, inc=1, device_id=device, device_id_type=MESH)
        pl.semaphore_signal(barrier, inc=1, device_id={**device, "tp": 1 - tp}, device_id_type=MESH)
    pl.semaphore_signal(barrier, inc=1, device_id={"tp": 1 - tp}, device_id_type=MESH)

    load_f = pltpu.make_async_copy(f_hbm, f_ref, load_sem.at[2])
    load_fm = pltpu.make_async_copy(fm_hbm, fm_ref, load_sem.at[3])
    load_sm = pltpu.make_async_copy(sm_hbm, sm_ref, load_sem.at[4])
    load_x = pltpu.make_async_copy(x_hbm, xv, load_sem.at[0])
    load_v = pltpu.make_async_copy(v_hbm, vv, load_sem.at[1])
    for load in (load_f, load_fm, load_sm, load_x, load_v):
        load.start()

    load_f.wait()
    fbuf[own_f] = f_ref[pl.ds(aligned(y, ROWS), ROWS), :]
    load_fm.wait()
    load_sm.wait()
    for px in range(NX):
        cols = pl.ds(aligned(y * NX + px, LANES), LANES)
        mom_send[px, 0:OWNED, :] = fm_ref[:, cols]
        mom_send[px, OWNED:2 * OWNED, :] = sm_ref[:, cols]
    cols = pl.ds(aligned(own, LANES), LANES)
    mom_recv[x, 0:OWNED, :] = fm_ref[:, cols]
    mom_recv[x, OWNED:2 * OWNED, :] = sm_ref[:, cols]

    pl.semaphore_wait(barrier, NZ - 1 + 2 * (PEERS - 1) + 1)

    def gather_z(buf, slot, send_sem, z_sem):
        for d in Z_FAR:
            i, k = GROUP_OF[NZ - d]
            dst = buf.at[BASE[i] + slot * len(GROUPS[i]) + k]
            send(buf.at[slot], dst, send_sem, z_sem.at[NZ - d], z_peer(d))

    def gather_plane(buf, slot, i, send_sem, z_sem, plane_sem):
        n = len(GROUPS[i])
        block = buf.at[pl.ds(BASE[i] + slot * n, n)]
        for d in GROUPS[i]:
            if d:
                drain(buf.at[0], z_sem.at[d])
        for dx, dy in PLANE:
            send(block, block, send_sem, plane_sem.at[i], plane_peer(dx, dy)[2])

    def arrived(buf, i, plane_sem):
        n = len(GROUPS[i])
        drain(buf.at[pl.ds(0, (PEERS - 1) * n)], plane_sem.at[i])
        return buf[BASE[i]:BASE[i] + PEERS * n].reshape(PEERS, n, ROWS, LANES)

    gather_z(fbuf, own_f, send_f, fz_sem)
    for i in range(len(GROUPS)):
        gather_plane(fbuf, own_f, i, send_f, fz_sem, fxy_sem)
    for dx in range(1, NX):
        px = lax.rem(x + dx, NX)
        send(mom_send.at[px], mom_recv.at[x], send_m, m_sem, {"fs": z * NX + px})

    load_x.wait()
    for i, group in enumerate(GROUPS):
        blocks = arrived(fbuf, i, fxy_sem)
        term = p_acc[...] if i else None
        for k, d in enumerate(group):
            columns = xv[:, pl.ds(aligned(lax.rem(z + d, NZ), ZBLOCK), ZBLOCK)]
            block = blocks[:, k].reshape(ZBLOCK, RANK)
            product = jnp.dot(columns, block, preferred_element_type=jnp.float32)
            term = product if term is None else term + product
        p_acc[...] = term
    projected = p_acc[...]
    upper = projected.astype(jnp.bfloat16)
    lower = (projected - upper.astype(jnp.float32)).astype(jnp.bfloat16)
    pt[0:RANK, :] = upper.T
    pt[RANK:, :] = lower.T

    def send_part(part, dy):
        begin = sum(len(p) for p in PARTS[:part])
        for dx in NEAR[::-1]:
            if dx or dy:
                px, py, device = plane_peer(dx, dy)
                src = lsend.at[py * NX + px, pl.ds(begin, len(PARTS[part]))]
                dst = lrecv.at[own, pl.ds(begin, len(PARTS[part]))]
                send(src, dst, send_l, lxy_sem.at[part], device)

    load_v.wait()
    chunks = [2, 1, 3, 0]
    for step, dy in enumerate(chunks):
        py = lax.rem(y + dy, NY)
        cols = pl.ds(aligned(py, NX * LANES), NX * LANES)
        both = jnp.dot(pt[...], vv[:, cols], preferred_element_type=jnp.float32)
        pt_terms = (both[0:RANK] + both[RANK:]).astype(jnp.bfloat16)
        terms = pt_terms.reshape(NZ, ROWS, NX * LANES)
        column[...] = terms
        for slot, d in enumerate(ORDER):
            rows = column[lax.rem(z + d, NZ)]
            for px in range(NX):
                lsend[py * NX + px, slot] = rows[:, px * LANES:(px + 1) * LANES]
        send_part(0, dy)
        if step == 2:
            send_part(1, chunks[0])
    for dy in chunks[1:]:
        send_part(1, dy)
    lrecv[own] = lsend[own]

    whole = fbuf[...].reshape(D, RANK)
    gram = lax.dot_general(whole, whole, (((0,), (0,)), ((), ())), preferred_element_type=jnp.float32)
    gram_1 = gram.astype(jnp.bfloat16)
    rest = gram - gram_1.astype(jnp.float32)
    gram_2 = rest.astype(jnp.bfloat16)
    gram_3 = (rest - gram_2.astype(jnp.float32)).astype(jnp.bfloat16)

    total = None
    for slot, d in enumerate(ORDER):
        for part, group in enumerate(PARTS):
            if d == group[0]:
                drain(lrecv.at[pl.ds(0, PEERS - 1), pl.ds(0, len(group))], lxy_sem.at[part])
        summed = jnp.sum(lrecv[:, slot].astype(jnp.float32), axis=0)
        if d:
            zsend[d] = summed.astype(jnp.bfloat16)
            send(zsend.at[d], zrecv.at[NZ - d], send_z, lz_sem.at[NZ - d], z_peer(d))
        else:
            total = summed
    drain(mom_recv.at[pl.ds(0, NX - 1)], m_sem)
    first = jnp.concatenate([mom_recv[i, 0:OWNED, :] for i in range(NX)], axis=0)
    second = jnp.concatenate([mom_recv[i, OWNED:2 * OWNED, :] for i in range(NX)], axis=0)
    for d in Z_FAR[::-1]:
        drain(zrecv.at[d], lz_sem.at[d])
        total = total + zrecv[d].astype(jnp.float32)

    new_first = first_decay * first + (1.0 - first_decay) * total
    new_second = second_decay * second + (1.0 - second_decay) * total * total
    ratio = new_first / (jnp.sqrt(new_second) + epsilon)
    rbuf[own] = ratio.astype(jnp.bfloat16)

    gather_z(rbuf, own, send_r, rz_sem)
    for i in range(len(GROUPS)):
        gather_plane(rbuf, own, i, send_r, rz_sem, rxy_sem)

    for d, (i, k) in GROUP_OF.items():
        column[lax.rem(z + d, NZ), :, 0:LANES] = rbuf[BASE[i] + own * len(GROUPS[i]) + k]
    tile = column[:, :, 0:LANES].reshape(RANK, LANES)
    mixed = (
        jnp.dot(gram_1, tile, preferred_element_type=jnp.float32)
        + jnp.dot(gram_2, tile, preferred_element_type=jnp.float32)
        + jnp.dot(gram_3, tile, preferred_element_type=jnp.float32)
    )
    square[...] = jnp.sum(mixed * tile.astype(jnp.float32), axis=0, keepdims=True)
    mine = squares.at[tp * PEERS + own]
    for dx, dy in PLANE:
        device = plane_peer(dx, dy)[2]
        send(square, mine, send_q, q_sem, device)
        send(square, mine, send_q, q_sem, {**device, "tp": 1 - tp})
    send(square, mine, send_q, q_sem, {"tp": 1 - tp})
    squares[tp * PEERS + own] = square[...]

    for i in range(NX):
        lg_send[i, 0:OWNED, :] = total[i * OWNED:(i + 1) * OWNED, :]
    lg_recv[own, 0:OWNED, :] = lg_send[x, 0:OWNED, :]
    for dx, dy in PLANE:
        px, py, device = plane_peer(dx, dy)
        send(lg_send.at[px], lg_recv.at[own], send_g, g_sem, device)

    for i, group in enumerate(GROUPS):
        blocks = arrived(rbuf, i, rxy_sem)
        for k, d in enumerate(group):
            rows = pl.ds(aligned(lax.rem(z + d, NZ), ROWS), ROWS)
            for j in range(PEERS):
                rat_out[rows, j * LANES:(j + 1) * LANES] = blocks[j, k]
    drain(squares.at[pl.ds(0, 2 * PEERS - 1)], q_sem)
    tot_out[...] = jnp.sum(squares[...], axis=0)
    drain(lg_recv.at[pl.ds(0, PEERS - 1)], g_sem)
    lg_out[...] = lg_recv[...]

    for buf, sem in ((fbuf, send_f), (rbuf, send_r)):
        drain(buf.at[pl.ds(0, NZ - 1)], sem)
        drain(buf.at[pl.ds(0, (PEERS - 1) * NZ)], sem)
    drain(lsend.at[pl.ds(0, PEERS - 1)], send_l)
    drain(zsend.at[pl.ds(0, NZ - 1)], send_z)
    drain(mom_send.at[pl.ds(0, NX - 1)], send_m)
    drain(lg_recv.at[pl.ds(0, PEERS - 1)], send_g)
    drain(squares.at[pl.ds(0, 2 * PEERS - 1)], send_q)


def exchange(saved_input, value_cotangent, factor, first_moment, second_moment):
    bf16, f32 = jnp.bfloat16, jnp.float32
    dma = pltpu.SemaphoreType.DMA
    vmem = pl.BlockSpec(memory_space=pltpu.VMEM)
    hbm = pl.BlockSpec(memory_space=pltpu.HBM)
    return pl.pallas_call(
        exchange_kernel,
        out_shape=(
            jax.ShapeDtypeStruct((RANK, COLS), bf16),
            jax.ShapeDtypeStruct((PEERS, 8, LANES), f32),
            jax.ShapeDtypeStruct((1, LANES), f32),
        ),
        in_specs=[hbm] * 5,
        out_specs=(vmem,) * 3,
        scratch_shapes=[
            pltpu.VMEM((D // (NX * NZ), RANK), bf16),
            pltpu.VMEM((OWNED, COLS), f32),
            pltpu.VMEM((OWNED, COLS), f32),
            pltpu.VMEM((TOKENS, D), bf16),
            pltpu.VMEM((TOKENS, COLS), bf16),
            pltpu.VMEM((NZ * PEERS, ROWS, LANES), bf16),
            pltpu.VMEM((TOKENS, RANK), f32),
            pltpu.VMEM((2 * RANK, TOKENS), bf16),
            pltpu.VMEM((PEERS, NZ, ROWS, LANES), bf16),
            pltpu.VMEM((PEERS, NZ, ROWS, LANES), bf16),
            pltpu.VMEM((NZ, ROWS, LANES), bf16),
            pltpu.VMEM((NZ, ROWS, LANES), bf16),
            pltpu.VMEM((NZ * PEERS, ROWS, LANES), bf16),
            pltpu.VMEM((NZ, ROWS, NX * LANES), bf16),
            pltpu.VMEM((NX, 8, LANES), f32),
            pltpu.VMEM((NX, 8, LANES), f32),
            pltpu.VMEM((NX, 8, LANES), f32),
            pltpu.VMEM((PEERS, 8, LANES), f32),
            pltpu.VMEM((1, LANES), f32),
            pltpu.VMEM((2 * PEERS, 1, LANES), f32),
            dma((5,)),
        ] + [dma] * 7 + [
            dma((NZ,)), dma((len(GROUPS),)), dma((len(PARTS),)), dma((NZ,)), dma((NZ,)), dma((len(GROUPS),)),
        ] + [dma] * 3,
        compiler_params=pltpu.CompilerParams(
            collective_id=0, has_side_effects=True, vmem_limit_bytes=32 * 2**20
        ),
    )(*(
        pltpu.with_memory_space_constraint(a, pltpu.HBM)
        for a in (saved_input, value_cotangent, factor, first_moment, second_moment)
    ))


def update_kernel(
    f_ref, rat_ref, lg_ref, tot_ref, w_ref, fm_ref, sm_ref,
    low_ref, first_ref, second_ref, dir_ref, weight_ref, copy_ref,
):
    total = jnp.sum(tot_ref[...], axis=(0, 1), keepdims=True)
    spread = jnp.sqrt(total / (D * E))
    raw = jnp.dot(f_ref[...], rat_ref[...], preferred_element_type=jnp.float32)
    direction = raw / (spread + 1.0)
    new_weight = w_ref[...] - learn_rate * direction
    dir_ref[...] = direction
    weight_ref[...] = new_weight
    copy_ref[...] = new_weight.astype(jnp.bfloat16)
    for j in range(PEERS):
        cols = slice(j * LANES, (j + 1) * LANES)
        low = lg_ref[j, 0:OWNED, :]
        low_ref[:, cols] = low
        first_ref[:, cols] = first_decay * fm_ref[:, cols] + (1.0 - first_decay) * low
        second_ref[:, cols] = second_decay * sm_ref[:, cols] + (1.0 - second_decay) * low * low


def update(factor, ratio, low, total, weight, first_moment, second_moment):
    f32 = jnp.float32
    rows = factor.shape[0]
    vmem = pl.BlockSpec(memory_space=pltpu.VMEM)
    small = jax.ShapeDtypeStruct((OWNED, COLS), f32)
    large = jax.ShapeDtypeStruct((rows, COLS), f32)
    return pl.pallas_call(
        update_kernel,
        out_shape=(small, small, small, large, large, jax.ShapeDtypeStruct((rows, COLS), jnp.bfloat16)),
        in_specs=[vmem] * 7,
        out_specs=(vmem,) * 6,
        compiler_params=pltpu.CompilerParams(vmem_limit_bytes=8 * 2**20),
    )(factor, ratio, low, total, weight, first_moment, second_moment)


def on_device(saved_input, value_cotangent, factor, weight, first_moment, second_moment):
    ratio, low, total = exchange(saved_input, value_cotangent, factor, first_moment, second_moment)
    return update(factor, ratio, low, total, weight, first_moment, second_moment)


def solution(mesh):
    placed = (
        P(("fs", "rep"), None),
        P(("fs", "rep"), "tp"),
        P("fs", None),
        P("fs", "tp"),
        P("fs", "tp"),
        P("fs", "tp"),
    )
    return jax.shard_map(
        on_device,
        mesh=mesh,
        in_specs=placed,
        out_specs=(P("fs", "tp"),) * 6,
        check_vma=False,
    )
```

time: 48.7 us -> 47.9 us (0.984)
  Pallas kernels: 47.9 us -> 47.1 us
    pallas_call x1, Pallas kernels: 46.6 us -> 45.8 us  [exchange(): pl.pallas_call(exchange_kernel, out_shape=(jax.ShapeDtypeStruct((RANK, CO...]
where the time goes in v3:
time: 47.9 us; the launch traced here: 47.8 us
  Pallas kernels  47.1 us (98%)
  between operations  0.7 us (1%)
    pallas_call x1, Pallas kernels, exchange(): pl.pallas_call(exchange_kernel, out_shape=(jax.ShapeDtypeStruct((RANK, CO...  45.8 us
    pallas_call x1, Pallas kernels, update(): pl.pallas_call(update_kernel, out_shape=(small, small, small, large, larg...  1.31 us

profile of v3, /device:TPU:1, one launch (start us, length us, event | category | flops | bytes accessed | tf_op | source)
XLA Modules:
  0.0 47.8 jit_solution(3842463805999011204)
XLA Ops:
  0.6 0.0 copy-start.2
  0.6 0.0 copy-start.1
  0.7 0.0 copy-start.3
  0.7 0.0 copy-start
  0.7 45.8 %shard_map.109 = (bf16[128,2048]{1,0:T(8,128)(2,1)S(1)}, f32[16,8,128]{2,1,0:T(8,128)S(1)}, f32[1,128]{1,0:T(1,128)S(1)}) custom-call(bf16[1024,2048]{1,0:T(8,128)(2,1)} %x_hbm.1, bf16[1024,2048]{1,0:T(8,128)(2,1)} %v_hbm.1, bf16[64,128]{1,0:T(8,128)(2,1)} %f_ref.1, f32[4,2048]{1,0:T(4,128)} %fm_ref.1, f32[4,2048]{1,0:T(4,128)} %sm_ref.1), custom_call_target="tpu_custom_call" | custom-call | tf_op jit(solution)/shard_map/pallas_call | solution.py:265
  46.4 0.0 copy-done.2
  46.4 0.0 copy-done.1
  46.5 0.0 copy-done.3
  46.5 0.0 copy-done
  46.5 1.3 %shard_map.110 = (f32[4,2048]{1,0:T(4,128)}, f32[4,2048]{1,0:T(4,128)}, f32[4,2048]{1,0:T(4,128)}, f32[64,2048]{1,0:T(8,128)}, f32[64,2048]{1,0:T(8,128)}, /*index=5*/bf16[64,2048]{1,0:T(8,128)(2,1)}) custom-call(bf16[64,128]{1,0:T(8,128)(2,1)S(1)} %copy-done.3, bf16[128,2048]{1,0:T(8,128)(2,1)S(1)} %get-tuple-element.9.rat_ref, ...), custom_call_target="tpu_custom_call" | custom-call | tf_op jit(solution)/shard_map/pallas_call | solution.py:334
Async XLA Ops:
  0.6 45.8 %copy-start.2 = (f32[4,2048]{1,0:T(4,128)S(1)}, f32[4,2048]{1,0:T(4,128)}, u32[]{:S(2)}) copy-start(f32[4,2048]{1,0:T(4,128)} %sm_ref.1) | copy-start | bytes 98308
  0.6 45.8 %copy-start.1 = (f32[4,2048]{1,0:T(4,128)S(1)}, f32[4,2048]{1,0:T(4,128)}, u32[]{:S(2)}) copy-start(f32[4,2048]{1,0:T(4,128)} %fm_ref.1) | copy-start | bytes 98308
  0.7 45.8 %copy-start.3 = (bf16[64,128]{1,0:T(8,128)(2,1)S(1)}, bf16[64,128]{1,0:T(8,128)(2,1)}, u32[]{:S(2)}) copy-start(bf16[64,128]{1,0:T(8,128)(2,1)} %f_ref.1) | copy-start | bytes 49156
  0.7 45.8 %copy-start = (f32[64,2048]{1,0:T(8,128)S(1)}, f32[64,2048]{1,0:T(8,128)}, u32[]{:S(2)}) copy-start(f32[64,2048]{1,0:T(8,128)} %w_ref.1) | copy-start | bytes 1572868

commit v4 on v3

--- a/solution.py
+++ b/solution.py
@@ -33,8 +33,8 @@
 GROUPS = [(0,), (1, 7), (2, 6), (3, 5), (4,)]
 BASE = [PEERS * sum(len(g) for g in GROUPS[:i]) for i in range(len(GROUPS))]
 GROUP_OF = {d: (i, k) for i, g in enumerate(GROUPS) for k, d in enumerate(g)}
-PARTS = [(4, 3, 5), (2, 6, 1, 7, 0)]
-ORDER = [d for part in PARTS for d in part]
+PIECES = 2
+PIECE = RANK // PIECES
 NEAR = [0, 3, 1, 2]
 
 
@@ -45,10 +45,10 @@
 def exchange_kernel(
     x_hbm, v_hbm, f_hbm, fm_hbm, sm_hbm,
     rat_out, lg_out, tot_out,
-    f_ref, fm_ref, sm_ref, xv, vv, fbuf, p_acc, pt, lsend, lrecv, zsend, zrecv, rbuf, column,
-    mom_send, mom_recv, lg_send, lg_recv, square, squares,
+    f_ref, fm_ref, sm_ref, xv, vv, fbuf, p_acc, pt, lsend, lrecv, zbuf, rbuf, low,
+    mom_own, mom_z, mom, lg_send, lg_recv, square, squares,
     load_sem, send_f, send_l, send_z, send_r, send_m, send_g, send_q,
-    fz_sem, fxy_sem, lxy_sem, lz_sem, rz_sem, rxy_sem, m_sem, g_sem, q_sem,
+    fz_sem, fxy_sem, lxy_sem, lz_sem, rxy_sem, mz_sem, mx_sem, g_sem, q_sem,
 ):
     fs = lax.axis_index("fs")
     y = lax.axis_index("rep")
@@ -98,11 +98,8 @@
     load_sm.wait()
     for px in range(NX):
         cols = pl.ds(aligned(y * NX + px, LANES), LANES)
-        mom_send[px, 0:OWNED, :] = fm_ref[:, cols]
-        mom_send[px, OWNED:2 * OWNED, :] = sm_ref[:, cols]
-    cols = pl.ds(aligned(own, LANES), LANES)
-    mom_recv[x, 0:OWNED, :] = fm_ref[:, cols]
-    mom_recv[x, OWNED:2 * OWNED, :] = sm_ref[:, cols]
+        mom_own[px, 0:OWNED, :] = fm_ref[:, cols]
+        mom_own[px, OWNED:2 * OWNED, :] = sm_ref[:, cols]
 
     pl.semaphore_wait(barrier, NZ - 1 + 2 * (PEERS - 1) + 1)
 
@@ -129,9 +126,9 @@
     gather_z(fbuf, own_f, send_f, fz_sem)
     for i in range(len(GROUPS)):
         gather_plane(fbuf, own_f, i, send_f, fz_sem, fxy_sem)
-    for dx in range(1, NX):
-        px = lax.rem(x + dx, NX)
-        send(mom_send.at[px], mom_recv.at[x], send_m, m_sem, {"fs": z * NX + px})
+    for d in Z_FAR:
+        send(mom_own, mom_z.at[:, z], send_m, mz_sem, z_peer(d))
+    mom_z[:, z] = mom_own[...]
 
     load_x.wait()
     for i, group in enumerate(GROUPS):
@@ -149,14 +146,15 @@
     pt[0:RANK, :] = upper.T
     pt[RANK:, :] = lower.T
 
-    def send_part(part, dy):
-        begin = sum(len(p) for p in PARTS[:part])
+    def rows_of(piece):
+        return pl.ds(piece * PIECE, PIECE)
+
+    def send_piece(piece, dy):
         for dx in NEAR[::-1]:
             if dx or dy:
                 px, py, device = plane_peer(dx, dy)
-                src = lsend.at[py * NX + px, pl.ds(begin, len(PARTS[part]))]
-                dst = lrecv.at[own, pl.ds(begin, len(PARTS[part]))]
-                send(src, dst, send_l, lxy_sem.at[part], device)
+                src = lsend.at[py * NX + px, rows_of(piece)]
+                send(src, lrecv.at[own, rows_of(piece)], send_l, lxy_sem.at[piece], device)
 
     load_v.wait()
     chunks = [2, 1, 3, 0]
@@ -164,19 +162,21 @@
         py = lax.rem(y + dy, NY)
         cols = pl.ds(aligned(py, NX * LANES), NX * LANES)
         both = jnp.dot(pt[...], vv[:, cols], preferred_element_type=jnp.float32)
-        pt_terms = (both[0:RANK] + both[RANK:]).astype(jnp.bfloat16)
-        terms = pt_terms.reshape(NZ, ROWS, NX * LANES)
-        column[...] = terms
-        for slot, d in enumerate(ORDER):
-            rows = column[lax.rem(z + d, NZ)]
-            for px in range(NX):
-                lsend[py * NX + px, slot] = rows[:, px * LANES:(px + 1) * LANES]
-        send_part(0, dy)
+        terms = (both[0:RANK] + both[RANK:]).astype(jnp.bfloat16)
+        for px in range(NX):
+            lsend[py * NX + px] = terms[:, px * LANES:(px + 1) * LANES]
+        send_piece(0, dy)
         if step == 2:
-            send_part(1, chunks[0])
+            send_piece(1, chunks[0])
     for dy in chunks[1:]:
-        send_part(1, dy)
+        send_piece(1, dy)
     lrecv[own] = lsend[own]
+
+    drain(mom_z.at[:, pl.ds(0, NZ - 1)], mz_sem)
+    for dx in range(1, NX):
+        px = lax.rem(x + dx, NX)
+        send(mom_z.at[px], mom.at[x], send_m, mx_sem, {"fs": z * NX + px})
+    mom[x] = mom_z[x]
 
     whole = fbuf[...].reshape(D, RANK)
     gram = lax.dot_general(whole, whole, (((0,), (0,)), ((), ())), preferred_element_type=jnp.float32)
@@ -185,36 +185,32 @@
     gram_2 = rest.astype(jnp.bfloat16)
     gram_3 = (rest - gram_2.astype(jnp.float32)).astype(jnp.bfloat16)
 
-    total = None
-    for slot, d in enumerate(ORDER):
-        for part, group in enumerate(PARTS):
-            if d == group[0]:
-                drain(lrecv.at[pl.ds(0, PEERS - 1), pl.ds(0, len(group))], lxy_sem.at[part])
-        summed = jnp.sum(lrecv[:, slot].astype(jnp.float32), axis=0)
-        if d:
-            zsend[d] = summed.astype(jnp.bfloat16)
-            send(zsend.at[d], zrecv.at[NZ - d], send_z, lz_sem.at[NZ - d], z_peer(d))
-        else:
-            total = summed
-    drain(mom_recv.at[pl.ds(0, NX - 1)], m_sem)
-    first = jnp.concatenate([mom_recv[i, 0:OWNED, :] for i in range(NX)], axis=0)
-    second = jnp.concatenate([mom_recv[i, OWNED:2 * OWNED, :] for i in range(NX)], axis=0)
-    for d in Z_FAR[::-1]:
-        drain(zrecv.at[d], lz_sem.at[d])
-        total = total + zrecv[d].astype(jnp.float32)
-
-    new_first = first_decay * first + (1.0 - first_decay) * total
-    new_second = second_decay * second + (1.0 - second_decay) * total * total
-    ratio = new_first / (jnp.sqrt(new_second) + epsilon)
-    rbuf[own] = ratio.astype(jnp.bfloat16)
-
-    gather_z(rbuf, own, send_r, rz_sem)
-    for i in range(len(GROUPS)):
-        gather_plane(rbuf, own, i, send_r, rz_sem, rxy_sem)
-
-    for d, (i, k) in GROUP_OF.items():
-        column[lax.rem(z + d, NZ), :, 0:LANES] = rbuf[BASE[i] + own * len(GROUPS[i]) + k]
-    tile = column[:, :, 0:LANES].reshape(RANK, LANES)
+    for piece in range(PIECES):
+        drain(lrecv.at[pl.ds(0, PEERS - 1), rows_of(piece)], lxy_sem.at[piece])
+        summed = jnp.sum(lrecv[:, piece * PIECE:(piece + 1) * PIECE].astype(jnp.float32), axis=0)
+        part = zbuf.at[z, rows_of(piece)]
+        zbuf[z, rows_of(piece)] = summed.astype(jnp.bfloat16)
+        for d in Z_FAR:
+            send(part, part, send_z, lz_sem.at[piece], z_peer(d))
+
+    drain(mom.at[pl.ds(0, NX - 1)], mx_sem)
+    per = PIECE // ROWS
+    for piece in range(PIECES):
+        drain(zbuf.at[pl.ds(0, NZ - 1), rows_of(piece)], lz_sem.at[piece])
+        total = jnp.sum(zbuf[:, piece * PIECE:(piece + 1) * PIECE].astype(jnp.float32), axis=0)
+        low[piece * per:(piece + 1) * per] = total.reshape(per, ROWS, LANES)
+        owners = [(i, zs) for zs in range(piece * per, (piece + 1) * per) for i in range(NX)]
+        first = jnp.concatenate([mom[i, zs, 0:OWNED] for i, zs in owners], axis=0)
+        second = jnp.concatenate([mom[i, zs, OWNED:2 * OWNED] for i, zs in owners], axis=0)
+        new_first = first_decay * first + (1.0 - first_decay) * total
+        new_second = second_decay * second + (1.0 - second_decay) * total * total
+        ratio = new_first / (jnp.sqrt(new_second) + epsilon)
+        rbuf[own, rows_of(piece)] = ratio.astype(jnp.bfloat16)
+        part = rbuf.at[own, rows_of(piece)]
+        for dx, dy in PLANE:
+            send(part, part, send_r, rxy_sem.at[piece], plane_peer(dx, dy)[2])
+
+    tile = rbuf[own]
     mixed = (
         jnp.dot(gram_1, tile, preferred_element_type=jnp.float32)
         + jnp.dot(gram_2, tile, preferred_element_type=jnp.float32)
@@ -229,30 +225,30 @@
     send(square, mine, send_q, q_sem, {"tp": 1 - tp})
     squares[tp * PEERS + own] = square[...]
 
+    own_rows = low[z]
     for i in range(NX):
-        lg_send[i, 0:OWNED, :] = total[i * OWNED:(i + 1) * OWNED, :]
+        lg_send[i, 0:OWNED, :] = own_rows[i * OWNED:(i + 1) * OWNED, :]
     lg_recv[own, 0:OWNED, :] = lg_send[x, 0:OWNED, :]
     for dx, dy in PLANE:
         px, py, device = plane_peer(dx, dy)
         send(lg_send.at[px], lg_recv.at[own], send_g, g_sem, device)
 
-    for i, group in enumerate(GROUPS):
-        blocks = arrived(rbuf, i, rxy_sem)
-        for k, d in enumerate(group):
-            rows = pl.ds(aligned(lax.rem(z + d, NZ), ROWS), ROWS)
-            for j in range(PEERS):
-                rat_out[rows, j * LANES:(j + 1) * LANES] = blocks[j, k]
+    for piece in range(PIECES):
+        drain(rbuf.at[pl.ds(0, PEERS - 1), rows_of(piece)], rxy_sem.at[piece])
+        for j in range(PEERS):
+            rat_out[rows_of(piece), j * LANES:(j + 1) * LANES] = rbuf[j, rows_of(piece)]
     drain(squares.at[pl.ds(0, 2 * PEERS - 1)], q_sem)
     tot_out[...] = jnp.sum(squares[...], axis=0)
     drain(lg_recv.at[pl.ds(0, PEERS - 1)], g_sem)
     lg_out[...] = lg_recv[...]
 
-    for buf, sem in ((fbuf, send_f), (rbuf, send_r)):
-        drain(buf.at[pl.ds(0, NZ - 1)], sem)
-        drain(buf.at[pl.ds(0, (PEERS - 1) * NZ)], sem)
+    drain(fbuf.at[pl.ds(0, NZ - 1)], send_f)
+    drain(fbuf.at[pl.ds(0, (PEERS - 1) * NZ)], send_f)
     drain(lsend.at[pl.ds(0, PEERS - 1)], send_l)
-    drain(zsend.at[pl.ds(0, NZ - 1)], send_z)
-    drain(mom_send.at[pl.ds(0, NX - 1)], send_m)
+    drain(zbuf.at[pl.ds(0, NZ - 1)], send_z)
+    drain(rbuf.at[pl.ds(0, PEERS - 1)], send_r)
+    drain(mom_z.at[:, pl.ds(0, NZ - 1)], send_m)
+    drain(mom.at[pl.ds(0, NX - 1)], send_m)
     drain(lg_recv.at[pl.ds(0, PEERS - 1)], send_g)
     drain(squares.at[pl.ds(0, 2 * PEERS - 1)], send_q)
 
@@ -280,22 +276,22 @@
             pltpu.VMEM((NZ * PEERS, ROWS, LANES), bf16),
             pltpu.VMEM((TOKENS, RANK), f32),
             pltpu.VMEM((2 * RANK, TOKENS), bf16),
-            pltpu.VMEM((PEERS, NZ, ROWS, LANES), bf16),
-            pltpu.VMEM((PEERS, NZ, ROWS, LANES), bf16),
-            pltpu.VMEM((NZ, ROWS, LANES), bf16),
-            pltpu.VMEM((NZ, ROWS, LANES), bf16),
-            pltpu.VMEM((NZ * PEERS, ROWS, LANES), bf16),
-            pltpu.VMEM((NZ, ROWS, NX * LANES), bf16),
+            pltpu.VMEM((PEERS, RANK, LANES), bf16),
+            pltpu.VMEM((PEERS, RANK, LANES), bf16),
+            pltpu.VMEM((NZ, RANK, LANES), bf16),
+            pltpu.VMEM((PEERS, RANK, LANES), bf16),
+            pltpu.VMEM((NZ, ROWS, LANES), f32),
             pltpu.VMEM((NX, 8, LANES), f32),
-            pltpu.VMEM((NX, 8, LANES), f32),
+            pltpu.VMEM((NX, NZ, 8, LANES), f32),
+            pltpu.VMEM((NX, NZ, 8, LANES), f32),
             pltpu.VMEM((NX, 8, LANES), f32),
             pltpu.VMEM((PEERS, 8, LANES), f32),
             pltpu.VMEM((1, LANES), f32),
             pltpu.VMEM((2 * PEERS, 1, LANES), f32),
             dma((5,)),
         ] + [dma] * 7 + [
-            dma((NZ,)), dma((len(GROUPS),)), dma((len(PARTS),)), dma((NZ,)), dma((NZ,)), dma((len(GROUPS),)),
-        ] + [dma] * 3,
+            dma((NZ,)), dma((len(GROUPS),)), dma((PIECES,)), dma((PIECES,)), dma((PIECES,)),
+        ] + [dma] * 4,
         compiler_params=pltpu.CompilerParams(
             collective_id=0, has_side_effects=True, vmem_limit_bytes=32 * 2**20
         ),

time: 47.9 us -> 45.5 us (0.950)
  Pallas kernels: 47.1 us -> 44.7 us
    pallas_call x1, Pallas kernels: 45.8 us -> 43.4 us  [exchange(): pl.pallas_call(exchange_kernel, out_shape=(jax.ShapeDtypeStruct((RANK, CO...]
where the time goes in v4:
time: 45.5 us; the launch traced here: 45.4 us
  Pallas kernels  44.7 us (98%)
  between operations  0.7 us (2%)
    pallas_call x1, Pallas kernels, exchange(): pl.pallas_call(exchange_kernel, out_shape=(jax.ShapeDtypeStruct((RANK, CO...  43.4 us
    pallas_call x1, Pallas kernels, update(): pl.pallas_call(update_kernel, out_shape=(small, small, small, large, larg...  1.31 us

profile of v4, /device:TPU:1, one launch (start us, length us, event | category | flops | bytes accessed | tf_op | source)
XLA Modules:
  0.0 45.4 jit_solution(2494172635389791699)
XLA Ops:
  0.6 0.0 copy-start.2
  0.6 0.0 copy-start.1
  0.7 0.0 copy-start.3
  0.7 0.0 copy-start
  0.7 43.4 %shard_map.109 = (bf16[128,2048]{1,0:T(8,128)(2,1)S(1)}, f32[16,8,128]{2,1,0:T(8,128)S(1)}, f32[1,128]{1,0:T(1,128)S(1)}) custom-call(bf16[1024,2048]{1,0:T(8,128)(2,1)} %x_hbm.1, bf16[1024,2048]{1,0:T(8,128)(2,1)} %v_hbm.1, bf16[64,128]{1,0:T(8,128)(2,1)} %f_ref.1, f32[4,2048]{1,0:T(4,128)} %fm_ref.1, f32[4,2048]{1,0:T(4,128)} %sm_ref.1), custom_call_target="tpu_custom_call" | custom-call | tf_op jit(solution)/shard_map/pallas_call | solution.py:261
  44.1 0.0 copy-done.2
  44.1 0.0 copy-done.1
  44.1 0.0 copy-done.3
  44.1 0.0 copy-done
  44.1 1.3 %shard_map.110 = (f32[4,2048]{1,0:T(4,128)}, f32[4,2048]{1,0:T(4,128)}, f32[4,2048]{1,0:T(4,128)}, f32[64,2048]{1,0:T(8,128)}, f32[64,2048]{1,0:T(8,128)}, /*index=5*/bf16[64,2048]{1,0:T(8,128)(2,1)}) custom-call(bf16[64,128]{1,0:T(8,128)(2,1)S(1)} %copy-done.3, bf16[128,2048]{1,0:T(8,128)(2,1)S(1)} %get-tuple-element.9.rat_ref, ...), custom_call_target="tpu_custom_call" | custom-call | tf_op jit(solution)/shard_map/pallas_call | solution.py:330
Async XLA Ops:
  0.6 43.4 %copy-start.2 = (f32[4,2048]{1,0:T(4,128)S(1)}, f32[4,2048]{1,0:T(4,128)}, u32[]{:S(2)}) copy-start(f32[4,2048]{1,0:T(4,128)} %sm_ref.1) | copy-start | bytes 98308
  0.6 43.4 %copy-start.1 = (f32[4,2048]{1,0:T(4,128)S(1)}, f32[4,2048]{1,0:T(4,128)}, u32[]{:S(2)}) copy-start(f32[4,2048]{1,0:T(4,128)} %fm_ref.1) | copy-start | bytes 98308
  0.7 43.4 %copy-start.3 = (bf16[64,128]{1,0:T(8,128)(2,1)S(1)}, bf16[64,128]{1,0:T(8,128)(2,1)}, u32[]{:S(2)}) copy-start(bf16[64,128]{1,0:T(8,128)(2,1)} %f_ref.1) | copy-start | bytes 49156
  0.7 43.4 %copy-start = (f32[64,2048]{1,0:T(8,128)S(1)}, f32[64,2048]{1,0:T(8,128)}, u32[]{:S(2)}) copy-start(f32[64,2048]{1,0:T(8,128)} %w_ref.1) | copy-start | bytes 1572868

commit v5 on v4

--- a/solution.py
+++ b/solution.py
@@ -33,9 +33,9 @@
 GROUPS = [(0,), (1, 7), (2, 6), (3, 5), (4,)]
 BASE = [PEERS * sum(len(g) for g in GROUPS[:i]) for i in range(len(GROUPS))]
 GROUP_OF = {d: (i, k) for i, g in enumerate(GROUPS) for k, d in enumerate(g)}
-PIECES = 2
+PIECES = 4
 PIECE = RANK // PIECES
-NEAR = [0, 3, 1, 2]
+FAR = [2, 1, 3, 0]
 
 
 def aligned(value, multiple):
@@ -46,7 +46,7 @@
     x_hbm, v_hbm, f_hbm, fm_hbm, sm_hbm,
     rat_out, lg_out, tot_out,
     f_ref, fm_ref, sm_ref, xv, vv, fbuf, p_acc, pt, lsend, lrecv, zbuf, rbuf, low,
-    mom_own, mom_z, mom, lg_send, lg_recv, square, squares,
+    mom_own, mom_z, mom, lg_send, lg_recv, square, squares, grams,
     load_sem, send_f, send_l, send_z, send_r, send_m, send_g, send_q,
     fz_sem, fxy_sem, lxy_sem, lz_sem, rxy_sem, mz_sem, mx_sem, g_sem, q_sem,
 ):
@@ -140,36 +140,39 @@
             product = jnp.dot(columns, block, preferred_element_type=jnp.float32)
             term = product if term is None else term + product
         p_acc[...] = term
-    projected = p_acc[...]
-    upper = projected.astype(jnp.bfloat16)
-    lower = (projected - upper.astype(jnp.float32)).astype(jnp.bfloat16)
-    pt[0:RANK, :] = upper.T
-    pt[RANK:, :] = lower.T
+    pt[...] = p_acc[...].astype(jnp.bfloat16).T
 
     def rows_of(piece):
         return pl.ds(piece * PIECE, PIECE)
 
-    def send_piece(piece, dy):
-        for dx in NEAR[::-1]:
-            if dx or dy:
-                px, py, device = plane_peer(dx, dy)
-                src = lsend.at[py * NX + px, rows_of(piece)]
-                send(src, lrecv.at[own, rows_of(piece)], send_l, lxy_sem.at[piece], device)
-
-    load_v.wait()
-    chunks = [2, 1, 3, 0]
-    for step, dy in enumerate(chunks):
+    def send_piece(piece, dy, near):
+        for dx in near:
+            px, py, device = plane_peer(dx, dy)
+            src = lsend.at[py * NX + px, rows_of(piece)]
+            send(src, lrecv.at[own, rows_of(piece)], send_l, lxy_sem.at[piece], device)
+
+    def terms_of(dy):
         py = lax.rem(y + dy, NY)
         cols = pl.ds(aligned(py, NX * LANES), NX * LANES)
-        both = jnp.dot(pt[...], vv[:, cols], preferred_element_type=jnp.float32)
-        terms = (both[0:RANK] + both[RANK:]).astype(jnp.bfloat16)
+        terms = jnp.dot(pt[...], vv[:, cols], preferred_element_type=jnp.float32)
         for px in range(NX):
-            lsend[py * NX + px] = terms[:, px * LANES:(px + 1) * LANES]
-        send_piece(0, dy)
-        if step == 2:
-            send_piece(1, chunks[0])
-    for dy in chunks[1:]:
-        send_piece(1, dy)
+            tile = terms[:, px * LANES:(px + 1) * LANES]
+            lsend[py * NX + px] = tile.astype(jnp.bfloat16)
+
+    load_v.wait()
+
+    @pl.loop(0, NY - 1)
+    def _(step):
+        dy = lax.rem(2 + 3 * step + 3 * lax.div(step * (step - 1), 2), NY)
+        terms_of(dy)
+        send_piece(0, dy, FAR)
+
+    terms_of(0)
+    send_piece(0, 0, FAR[:-1])
+    for piece in range(1, PIECES):
+        for dy in (2, 1, 3):
+            send_piece(piece, dy, FAR)
+        send_piece(piece, 0, FAR[:-1])
     lrecv[own] = lsend[own]
 
     drain(mom_z.at[:, pl.ds(0, NZ - 1)], mz_sem)
@@ -184,6 +187,9 @@
     rest = gram - gram_1.astype(jnp.float32)
     gram_2 = rest.astype(jnp.bfloat16)
     gram_3 = (rest - gram_2.astype(jnp.float32)).astype(jnp.bfloat16)
+    grams[0:RANK] = gram_1
+    grams[RANK:2 * RANK] = gram_2
+    grams[2 * RANK:] = gram_3
 
     for piece in range(PIECES):
         drain(lrecv.at[pl.ds(0, PEERS - 1), rows_of(piece)], lxy_sem.at[piece])
@@ -211,11 +217,8 @@
             send(part, part, send_r, rxy_sem.at[piece], plane_peer(dx, dy)[2])
 
     tile = rbuf[own]
-    mixed = (
-        jnp.dot(gram_1, tile, preferred_element_type=jnp.float32)
-        + jnp.dot(gram_2, tile, preferred_element_type=jnp.float32)
-        + jnp.dot(gram_3, tile, preferred_element_type=jnp.float32)
-    )
+    mixed = jnp.dot(grams[...], tile, preferred_element_type=jnp.float32)
+    mixed = mixed[0:RANK] + mixed[RANK:2 * RANK] + mixed[2 * RANK:]
     square[...] = jnp.sum(mixed * tile.astype(jnp.float32), axis=0, keepdims=True)
     mine = squares.at[tp * PEERS + own]
     for dx, dy in PLANE:
@@ -275,7 +278,7 @@
             pltpu.VMEM((TOKENS, COLS), bf16),
             pltpu.VMEM((NZ * PEERS, ROWS, LANES), bf16),
             pltpu.VMEM((TOKENS, RANK), f32),
-            pltpu.VMEM((2 * RANK, TOKENS), bf16),
+            pltpu.VMEM((RANK, TOKENS), bf16),
             pltpu.VMEM((PEERS, RANK, LANES), bf16),
             pltpu.VMEM((PEERS, RANK, LANES), bf16),
             pltpu.VMEM((NZ, RANK, LANES), bf16),
@@ -288,6 +291,7 @@
             pltpu.VMEM((PEERS, 8, LANES), f32),
             pltpu.VMEM((1, LANES), f32),
             pltpu.VMEM((2 * PEERS, 1, LANES), f32),
+            pltpu.VMEM((3 * RANK, RANK), bf16),
             dma((5,)),
         ] + [dma] * 7 + [
             dma((NZ,)), dma((len(GROUPS),)), dma((PIECES,)), dma((PIECES,)), dma((PIECES,)),

time: 45.5 us -> 43.5 us (0.956)
  Pallas kernels: 44.7 us -> 42.7 us
    pallas_call x1, Pallas kernels: 43.4 us -> 41.4 us  [exchange(): pl.pallas_call(exchange_kernel, out_shape=(jax.ShapeDtypeStruct((RANK, CO...]
where the time goes in v5:
time: 43.5 us; the launch traced here: 43.4 us
  Pallas kernels  42.7 us (98%)
  between operations  0.7 us (2%)
    pallas_call x1, Pallas kernels, exchange(): pl.pallas_call(exchange_kernel, out_shape=(jax.ShapeDtypeStruct((RANK, CO...  41.4 us
    pallas_call x1, Pallas kernels, update(): pl.pallas_call(update_kernel, out_shape=(small, small, small, large, larg...  1.31 us

profile of v5, /device:TPU:1, one launch (start us, length us, event | category | flops | bytes accessed | tf_op | source)
XLA Modules:
  0.0 43.4 jit_solution(10343877141138028814)
XLA Ops:
  0.6 0.0 copy-start.2
  0.6 0.0 copy-start.1
  0.7 0.0 copy-start.3
  0.7 0.0 copy-start
  0.7 41.4 %shard_map.109 = (bf16[128,2048]{1,0:T(8,128)(2,1)S(1)}, f32[16,8,128]{2,1,0:T(8,128)S(1)}, f32[1,128]{1,0:T(1,128)S(1)}) custom-call(bf16[1024,2048]{1,0:T(8,128)(2,1)} %x_hbm.1, bf16[1024,2048]{1,0:T(8,128)(2,1)} %v_hbm.1, bf16[64,128]{1,0:T(8,128)(2,1)} %f_ref.1, f32[4,2048]{1,0:T(4,128)} %fm_ref.1, f32[4,2048]{1,0:T(4,128)} %sm_ref.1), custom_call_target="tpu_custom_call" | custom-call | tf_op jit(solution)/shard_map/pallas_call | solution.py:264
  42.1 0.0 copy-done.2
  42.1 0.0 copy-done.1
  42.1 0.0 copy-done.3
  42.1 0.0 copy-done
  42.1 1.3 %shard_map.110 = (f32[4,2048]{1,0:T(4,128)}, f32[4,2048]{1,0:T(4,128)}, f32[4,2048]{1,0:T(4,128)}, f32[64,2048]{1,0:T(8,128)}, f32[64,2048]{1,0:T(8,128)}, /*index=5*/bf16[64,2048]{1,0:T(8,128)(2,1)}) custom-call(bf16[64,128]{1,0:T(8,128)(2,1)S(1)} %copy-done.3, bf16[128,2048]{1,0:T(8,128)(2,1)S(1)} %get-tuple-element.9.rat_ref, ...), custom_call_target="tpu_custom_call" | custom-call | tf_op jit(solution)/shard_map/pallas_call | solution.py:334
Async XLA Ops:
  0.6 41.4 %copy-start.2 = (f32[4,2048]{1,0:T(4,128)S(1)}, f32[4,2048]{1,0:T(4,128)}, u32[]{:S(2)}) copy-start(f32[4,2048]{1,0:T(4,128)} %sm_ref.1) | copy-start | bytes 98308
  0.6 41.4 %copy-start.1 = (f32[4,2048]{1,0:T(4,128)S(1)}, f32[4,2048]{1,0:T(4,128)}, u32[]{:S(2)}) copy-start(f32[4,2048]{1,0:T(4,128)} %fm_ref.1) | copy-start | bytes 98308
  0.7 41.4 %copy-start.3 = (bf16[64,128]{1,0:T(8,128)(2,1)S(1)}, bf16[64,128]{1,0:T(8,128)(2,1)}, u32[]{:S(2)}) copy-start(bf16[64,128]{1,0:T(8,128)(2,1)} %f_ref.1) | copy-start | bytes 49156
  0.7 41.4 %copy-start = (f32[64,2048]{1,0:T(8,128)S(1)}, f32[64,2048]{1,0:T(8,128)}, u32[]{:S(2)}) copy-start(f32[64,2048]{1,0:T(8,128)} %w_ref.1) | copy-start | bytes 1572868

commit v6 on v5

--- a/solution.py
+++ b/solution.py
@@ -33,8 +33,10 @@
 GROUPS = [(0,), (1, 7), (2, 6), (3, 5), (4,)]
 BASE = [PEERS * sum(len(g) for g in GROUPS[:i]) for i in range(len(GROUPS))]
 GROUP_OF = {d: (i, k) for i, g in enumerate(GROUPS) for k, d in enumerate(g)}
-PIECES = 4
-PIECE = RANK // PIECES
+SIZES = [64, 32, 32]
+PIECES = len(SIZES)
+STARTS = [sum(SIZES[:i]) for i in range(PIECES)]
+AHEAD = 0
 FAR = [2, 1, 3, 0]
 
 
@@ -143,7 +145,7 @@
     pt[...] = p_acc[...].astype(jnp.bfloat16).T
 
     def rows_of(piece):
-        return pl.ds(piece * PIECE, PIECE)
+        return pl.ds(STARTS[piece], SIZES[piece])
 
     def send_piece(piece, dy, near):
         for dx in near:
@@ -193,38 +195,44 @@
 
     for piece in range(PIECES):
         drain(lrecv.at[pl.ds(0, PEERS - 1), rows_of(piece)], lxy_sem.at[piece])
-        summed = jnp.sum(lrecv[:, piece * PIECE:(piece + 1) * PIECE].astype(jnp.float32), axis=0)
+        summed = jnp.sum(lrecv[:, rows_of(piece)].astype(jnp.float32), axis=0)
         part = zbuf.at[z, rows_of(piece)]
         zbuf[z, rows_of(piece)] = summed.astype(jnp.bfloat16)
         for d in Z_FAR:
             send(part, part, send_z, lz_sem.at[piece], z_peer(d))
 
     drain(mom.at[pl.ds(0, NX - 1)], mx_sem)
-    per = PIECE // ROWS
     for piece in range(PIECES):
         drain(zbuf.at[pl.ds(0, NZ - 1), rows_of(piece)], lz_sem.at[piece])
-        total = jnp.sum(zbuf[:, piece * PIECE:(piece + 1) * PIECE].astype(jnp.float32), axis=0)
-        low[piece * per:(piece + 1) * per] = total.reshape(per, ROWS, LANES)
-        owners = [(i, zs) for zs in range(piece * per, (piece + 1) * per) for i in range(NX)]
+        total = jnp.sum(zbuf[:, rows_of(piece)].astype(jnp.float32), axis=0)
+        begin, end = STARTS[piece] // ROWS, (STARTS[piece] + SIZES[piece]) // ROWS
+        low[begin:end] = total.reshape(end - begin, ROWS, LANES)
+        owners = [(i, zs) for zs in range(begin, end) for i in range(NX)]
         first = jnp.concatenate([mom[i, zs, 0:OWNED] for i, zs in owners], axis=0)
         second = jnp.concatenate([mom[i, zs, OWNED:2 * OWNED] for i, zs in owners], axis=0)
         new_first = first_decay * first + (1.0 - first_decay) * total
         new_second = second_decay * second + (1.0 - second_decay) * total * total
         ratio = new_first / (jnp.sqrt(new_second) + epsilon)
-        rbuf[own, rows_of(piece)] = ratio.astype(jnp.bfloat16)
+        narrow = ratio.astype(jnp.bfloat16)
+        rbuf[own, rows_of(piece)] = narrow
         part = rbuf.at[own, rows_of(piece)]
-        for dx, dy in PLANE:
+        last = piece == PIECES - 1
+        for dx, dy in PLANE[:AHEAD] if last else PLANE:
             send(part, part, send_r, rxy_sem.at[piece], plane_peer(dx, dy)[2])
+        weights = grams[:, rows_of(piece)]
+        product = jnp.dot(weights, narrow, preferred_element_type=jnp.float32)
+        product = product[0:RANK] + product[RANK:2 * RANK] + product[2 * RANK:]
+        mixed = product if piece == 0 else mixed + product
 
     tile = rbuf[own]
-    mixed = jnp.dot(grams[...], tile, preferred_element_type=jnp.float32)
-    mixed = mixed[0:RANK] + mixed[RANK:2 * RANK] + mixed[2 * RANK:]
     square[...] = jnp.sum(mixed * tile.astype(jnp.float32), axis=0, keepdims=True)
     mine = squares.at[tp * PEERS + own]
-    for dx, dy in PLANE:
+    for i, (dx, dy) in enumerate(PLANE):
         device = plane_peer(dx, dy)[2]
         send(square, mine, send_q, q_sem, device)
         send(square, mine, send_q, q_sem, {**device, "tp": 1 - tp})
+        if i >= AHEAD:
+            send(part, part, send_r, rxy_sem.at[PIECES - 1], device)
     send(square, mine, send_q, q_sem, {"tp": 1 - tp})
     squares[tp * PEERS + own] = square[...]
 
@@ -307,35 +315,55 @@
 
 def update_kernel(
     f_ref, rat_ref, lg_ref, tot_ref, w_ref, fm_ref, sm_ref,
-    low_ref, first_ref, second_ref, dir_ref, weight_ref, copy_ref,
+    low_hbm, first_hbm, second_hbm, dir_hbm, weight_hbm, copy_hbm,
+    low_ref, first_ref, second_ref, dir_ref, weight_ref, copy_ref, sem,
 ):
+    saves = []
+
+    def save(src, dst):
+        copy = pltpu.make_async_copy(src, dst, sem.at[len(saves)])
+        copy.start()
+        saves.append(copy)
+
     total = jnp.sum(tot_ref[...], axis=(0, 1), keepdims=True)
-    spread = jnp.sqrt(total / (D * E))
-    raw = jnp.dot(f_ref[...], rat_ref[...], preferred_element_type=jnp.float32)
-    direction = raw / (spread + 1.0)
-    new_weight = w_ref[...] - learn_rate * direction
-    dir_ref[...] = direction
-    weight_ref[...] = new_weight
-    copy_ref[...] = new_weight.astype(jnp.bfloat16)
+    scale = 1.0 / (jnp.sqrt(total / (D * E)) + 1.0)
+    for begin, end in ((0, 32), (32, 64)):
+        rows = slice(begin, end)
+        at = pl.ds(begin, end - begin)
+        raw = jnp.dot(f_ref[rows], rat_ref[...], preferred_element_type=jnp.float32)
+        direction = raw * scale
+        dir_ref[rows] = direction
+        save(dir_ref.at[at], dir_hbm.at[at])
+        new_weight = w_ref[rows] - learn_rate * direction
+        weight_ref[rows] = new_weight
+        save(weight_ref.at[at], weight_hbm.at[at])
+        copy_ref[rows] = new_weight.astype(jnp.bfloat16)
+        save(copy_ref.at[at], copy_hbm.at[at])
     for j in range(PEERS):
         cols = slice(j * LANES, (j + 1) * LANES)
         low = lg_ref[j, 0:OWNED, :]
         low_ref[:, cols] = low
         first_ref[:, cols] = first_decay * fm_ref[:, cols] + (1.0 - first_decay) * low
         second_ref[:, cols] = second_decay * sm_ref[:, cols] + (1.0 - second_decay) * low * low
+    save(low_ref, low_hbm)
+    save(first_ref, first_hbm)
+    save(second_ref, second_hbm)
+    for copy in saves:
+        copy.wait()
 
 
 def update(factor, ratio, low, total, weight, first_moment, second_moment):
-    f32 = jnp.float32
+    f32, bf16 = jnp.float32, jnp.bfloat16
     rows = factor.shape[0]
     vmem = pl.BlockSpec(memory_space=pltpu.VMEM)
-    small = jax.ShapeDtypeStruct((OWNED, COLS), f32)
-    large = jax.ShapeDtypeStruct((rows, COLS), f32)
+    hbm = pl.BlockSpec(memory_space=pltpu.HBM)
+    shapes = [((OWNED, COLS), f32)] * 3 + [((rows, COLS), f32)] * 2 + [((rows, COLS), bf16)]
     return pl.pallas_call(
         update_kernel,
-        out_shape=(small, small, small, large, large, jax.ShapeDtypeStruct((rows, COLS), jnp.bfloat16)),
+        out_shape=tuple(jax.ShapeDtypeStruct(*s) for s in shapes),
         in_specs=[vmem] * 7,
-        out_specs=(vmem,) * 6,
+        out_specs=(hbm,) * 6,
+        scratch_shapes=[pltpu.VMEM(*s) for s in shapes] + [pltpu.SemaphoreType.DMA((9,))],
         compiler_params=pltpu.CompilerParams(vmem_limit_bytes=8 * 2**20),
     )(factor, ratio, low, total, weight, first_moment, second_moment)
 

time: 43.5 us -> 42.7 us (0.982)
  Pallas kernels: 42.7 us -> 41.9 us
    pallas_call x1, Pallas kernels: 41.4 us -> 40.5 us  [exchange(): pl.pallas_call(exchange_kernel, out_shape=(jax.ShapeDtypeStruct((RANK, CO...]
where the time goes in v6:
time: 42.7 us; the launch traced here: 42.6 us
  Pallas kernels  41.9 us (98%)
  between operations  0.7 us (2%)
    pallas_call x1, Pallas kernels, exchange(): pl.pallas_call(exchange_kernel, out_shape=(jax.ShapeDtypeStruct((RANK, CO...  40.5 us
    pallas_call x1, Pallas kernels, update(): pl.pallas_call(update_kernel, out_shape=tuple((jax.ShapeDtypeStruct(*s) f...  1.36 us

profile of v6, /device:TPU:1, one launch (start us, length us, event | category | flops | bytes accessed | tf_op | source)
XLA Modules:
  0.0 42.6 jit_solution(4969990649431401352)
XLA Ops:
  0.6 0.0 copy-start.2
  0.6 0.0 copy-start.1
  0.7 0.0 copy-start.3
  0.7 0.0 copy-start
  0.7 40.5 %shard_map.109 = (bf16[128,2048]{1,0:T(8,128)(2,1)S(1)}, f32[16,8,128]{2,1,0:T(8,128)S(1)}, f32[1,128]{1,0:T(1,128)S(1)}) custom-call(bf16[1024,2048]{1,0:T(8,128)(2,1)} %x_hbm.1, bf16[1024,2048]{1,0:T(8,128)(2,1)} %v_hbm.1, bf16[64,128]{1,0:T(8,128)(2,1)} %f_ref.1, f32[4,2048]{1,0:T(4,128)} %fm_ref.1, f32[4,2048]{1,0:T(4,128)} %sm_ref.1), custom_call_target="tpu_custom_call" | custom-call | tf_op jit(solution)/shard_map/pallas_call | solution.py:272
  41.2 0.0 copy-done.2
  41.2 0.0 copy-done.1
  41.2 0.0 copy-done.3
  41.2 0.0 copy-done
  41.2 1.4 %shard_map.110 = (f32[4,2048]{1,0:T(4,128)}, f32[4,2048]{1,0:T(4,128)}, f32[4,2048]{1,0:T(4,128)}, f32[64,2048]{1,0:T(8,128)}, f32[64,2048]{1,0:T(8,128)}, /*index=5*/bf16[64,2048]{1,0:T(8,128)(2,1)}) custom-call(bf16[64,128]{1,0:T(8,128)(2,1)S(1)} %copy-done.3, bf16[128,2048]{1,0:T(8,128)(2,1)S(1)} %get-tuple-element.9.rat_ref, ...), custom_call_target="tpu_custom_call" | custom-call | tf_op jit(solution)/shard_map/pallas_call | solution.py:361
Async XLA Ops:
  0.6 40.5 %copy-start.2 = (f32[4,2048]{1,0:T(4,128)S(1)}, f32[4,2048]{1,0:T(4,128)}, u32[]{:S(2)}) copy-start(f32[4,2048]{1,0:T(4,128)} %sm_ref.1) | copy-start | bytes 98308
  0.6 40.5 %copy-start.1 = (f32[4,2048]{1,0:T(4,128)S(1)}, f32[4,2048]{1,0:T(4,128)}, u32[]{:S(2)}) copy-start(f32[4,2048]{1,0:T(4,128)} %fm_ref.1) | copy-start | bytes 98308
  0.7 40.5 %copy-start.3 = (bf16[64,128]{1,0:T(8,128)(2,1)S(1)}, bf16[64,128]{1,0:T(8,128)(2,1)}, u32[]{:S(2)}) copy-start(bf16[64,128]{1,0:T(8,128)(2,1)} %f_ref.1) | copy-start | bytes 49156
  0.7 40.5 %copy-start = (f32[64,2048]{1,0:T(8,128)S(1)}, f32[64,2048]{1,0:T(8,128)}, u32[]{:S(2)}) copy-start(f32[64,2048]{1,0:T(8,128)} %w_ref.1) | copy-start | bytes 1572868
